TPU v7x, 32 devices: a whole 2x2x4 slice. The times are simulated.
32 devices in a mesh: sp: 4 (over y, x), tp: 8 (over z, core).
Axes of the slice: x: 2, y: 2, z: 4, core: 2. Of those that a mesh axis runs over, the one named last changes fastest.
Arguments:
- queries: bfloat16 [2048, 1536], P('sp', 'tp'), may hold values from -34 to 34
- latent: bfloat16 [2048, 512], P('sp'), may hold values from -6 to 6
- rot_key: bfloat16 [2048, 32], P('sp'), may hold values from -34 to 34
- latent_gain: float32 [512], replicated, may hold values from 0.1 to 1.9
- key_up: bfloat16 [512, 1024], P(None, 'tp'), may hold values from -0.25 to 0.25
- value_up: bfloat16 [512, 1024], P(None, 'tp'), may hold values from -0.70710678 to 0.70710678
- query_gain: float32 [96], replicated, may hold values from 0.5 to 6
- key_gain: float32 [96], replicated, may hold values from 0.5 to 6
- out_gain: float32 [1024], replicated, may hold values from 0.1 to 1.9
- out_weight: bfloat16 [1024, 2048], replicated, may hold values from -0.1875 to 0.1875
- residual: bfloat16 [2048, 2048], P(('sp', 'tp')), may hold values from -6 to 6
- ffn_gain: float32 [2048], replicated, may hold values from 0.1 to 1.9
- routes: int32 [2048, 2], P(('sp', 'tp')), may hold values from 0 to 3, all different within a row; in each aligned block of 64 rows (0 to 63, 64 to 127, ...) at most 36 rows name the same one
- route_weights: float32 [2048, 2], P(('sp', 'tp')), may hold values from 0.2 to 1
- expert_gate: bfloat16 [4, 2048, 2048], P('sp', None, 'tp'), may hold values from -0.125 to 0.125
- expert_up: bfloat16 [4, 2048, 2048], P('sp', None, 'tp'), may hold values from -0.125 to 0.125
- expert_down: bfloat16 [4, 2048, 2048], P('sp', 'tp'), may hold values from -0.125 to 0.125
Outputs:
- layer_out: bfloat16 [2048, 2048], P(('sp', 'tp'))
Inputs may be any that keep to these rules, and one draw needn't show every extreme that they name: `routes`: the 2 experts of a token differ. Among the 64 rows of one device each expert is named by at most 36 rows, a bound that some block reaches.
All inputs are finite; a program needn't handle non-finite values.
Results may differ from a plain program's by a relative error of at most 0.02.
The roundings to bfloat16 on the way count: a program that leaves them out, or rounds other values in their place, can miss the bound.
Values may be sent and summed in bfloat16 or wider, within the bound.
A program may use at most 128 MiB of HBM per device.

v0:
```python
import jax
import jax.numpy as jnp
from jax import lax
from jax.sharding import PartitionSpec as P

D = 2048
NOPE = 64
ROPE = 32
VH = 64
TOPK = 2
QK = 96


epsilon = 1e-06
rope_base = 10000.0


def rms_scale(values):
    return lax.rsqrt(jnp.mean(values * values, axis=-1, keepdims=True) + epsilon)


def rotate_half(values, angles):
    half_dims = values.shape[-1] // 2
    first_half = values[..., :half_dims]
    second_half = values[..., half_dims:]
    cosine = jnp.cos(angles)
    sine_val = jnp.sin(angles)
    return jnp.concatenate(
        [
            first_half * cosine - second_half * sine_val,
            second_half * cosine + first_half * sine_val,
        ],
        axis=-1,
    )


def head_prepare(raw_rows, gain_vec, angles):
    normed_rows = raw_rows * rms_scale(raw_rows) * gain_vec
    turned_rows = rotate_half(normed_rows[..., NOPE:], angles[:, None, :])
    return jnp.concatenate([normed_rows[..., :NOPE], turned_rows], axis=-1).astype(jnp.bfloat16)


def slot_targets(route_rows, expert_total, slot_cap):
    flat_routes = route_rows.reshape(-1)
    one_hot = (flat_routes[:, None] == jnp.arange(expert_total, dtype=jnp.int32)[None, :]).astype(
        jnp.int32
    )
    earlier = jnp.cumsum(one_hot, axis=0) - one_hot
    rank_in = jnp.sum(earlier * one_hot, axis=1)
    return (flat_routes * slot_cap + rank_in).reshape(route_rows.shape)


def select_matrix(targets, slot_total):
    hits = targets[:, :, None] == jnp.arange(slot_total, dtype=jnp.int32)[None, None, :]
    return jnp.sum(hits.astype(jnp.bfloat16), axis=1)


def shards(
    queries,
    latent,
    rot_key,
    latent_gain,
    key_up,
    value_up,
    query_gain,
    key_gain,
    out_gain,
    out_weight,
    residual,
    ffn_gain,
    routes,
    route_weights,
    expert_gate,
    expert_up,
    expert_down,
):
    shard_len = queries.shape[0]
    local_heads = key_up.shape[1] // NOPE
    sp_count = lax.axis_size("sp")
    tp_count = lax.axis_size("tp")
    my_first = lax.axis_index("sp") * shard_len
    my_last = my_first + shard_len - 1
    positions = my_first + jnp.arange(shard_len, dtype=jnp.int32)
    inverse = rope_base ** (-jnp.arange(0, ROPE, 2, dtype=jnp.float32) / ROPE)
    angles = positions.astype(jnp.float32)[:, None] * inverse[None, :]
    lat_f32 = latent.astype(jnp.float32)
    normed_latent = (lat_f32 * rms_scale(lat_f32) * latent_gain).astype(jnp.bfloat16)
    key_nope = jnp.dot(normed_latent, key_up, preferred_element_type=jnp.float32).astype(
        jnp.bfloat16
    )
    value_rows = jnp.dot(normed_latent, value_up, preferred_element_type=jnp.float32).astype(
        jnp.bfloat16
    )
    shared = jnp.broadcast_to(
        rot_key.astype(jnp.float32)[:, None, :], (shard_len, local_heads, ROPE)
    )
    raw_keys = jnp.concatenate(
        [key_nope.astype(jnp.float32).reshape(shard_len, local_heads, NOPE), shared], axis=-1
    )
    key_rows = head_prepare(raw_keys, key_gain, angles)
    query_rows = head_prepare(
        queries.astype(jnp.float32).reshape(shard_len, local_heads, QK), query_gain, angles
    )
    query_heads = jnp.transpose(query_rows, (1, 0, 2))
    bundle = jnp.concatenate(
        [
            jnp.transpose(key_rows, (1, 2, 0)),
            jnp.transpose(value_rows.reshape(shard_len, local_heads, VH), (1, 2, 0)),
        ],
        axis=1,
    )
    score_scale = QK ** (-0.5)
    init_state = (
        jnp.full((local_heads, shard_len), -1e30, jnp.float32),
        jnp.zeros((local_heads, shard_len), jnp.float32),
        jnp.zeros((local_heads, shard_len, VH), jnp.float32),
    )
    key_piece = lax.all_gather(bundle, "sp", axis=2, tiled=True)
    block_count = key_piece.shape[2] // shard_len

    def one_block(block_index, running_state):
        first_key = block_index * shard_len

        def compute(inner):
            row_peak, row_total, weighted = inner
            key_part = lax.dynamic_slice_in_dim(key_piece, block_index * shard_len, shard_len, 2)
            scores = (
                jnp.einsum(
                    "hqc,hck->hqk",
                    query_heads,
                    key_part[:, :QK, :],
                    preferred_element_type=jnp.float32,
                )
                * score_scale
            )
            key_pos = first_key + jnp.arange(shard_len, dtype=jnp.int32)
            allowed = key_pos[None, None, :] <= positions[None, :, None]
            scores = jnp.where(allowed, scores, -1e30)
            new_peak = jnp.maximum(row_peak, jnp.max(scores, axis=2))
            exponent = jnp.where(allowed, jnp.exp(scores - new_peak[..., None]), 0.0)
            factor = jnp.exp(row_peak - new_peak)
            new_total = row_total * factor + jnp.sum(exponent, axis=2)
            contrib = jnp.einsum(
                "hqk,hvk->hqv",
                exponent.astype(jnp.bfloat16),
                key_part[:, QK:, :],
                preferred_element_type=jnp.float32,
            )
            return (new_peak, new_total, weighted * factor[..., None] + contrib)

        return lax.cond(first_key <= my_last, compute, lambda inner: inner, running_state)

    row_peak, row_total, weighted = lax.fori_loop(0, block_count, one_block, init_state)
    attended = (weighted / row_total[..., None]).astype(jnp.bfloat16)
    tok_count = residual.shape[0]
    head_major = jnp.transpose(attended, (1, 0, 2)).reshape(shard_len, local_heads * VH)
    token_rows = lax.all_to_all(head_major, "tp", split_axis=0, concat_axis=1, tiled=True).astype(
        jnp.float32
    )
    normed_rows = (token_rows * rms_scale(token_rows) * out_gain).astype(jnp.bfloat16)
    partials = jnp.einsum(
        "tgc,gcd->tgd",
        normed_rows.reshape(tok_count, tp_count, -1),
        out_weight.reshape(tp_count, -1, D),
        preferred_element_type=jnp.float32,
    )
    rounded = lax.optimization_barrier(partials.astype(jnp.bfloat16))
    mixed = jnp.sum(rounded.astype(jnp.float32), axis=1)
    middle = residual.astype(jnp.float32) + mixed
    ffn_input = (middle * rms_scale(middle) * ffn_gain).astype(jnp.bfloat16)
    slot_cap = max(2, 9 * tok_count * TOPK // (8 * sp_count))
    slot_total = sp_count * slot_cap
    targets = slot_targets(routes, sp_count, slot_cap)
    chooser = select_matrix(targets, slot_total)
    outbound = (
        jnp.einsum("ts,td->sd", chooser, ffn_input, preferred_element_type=jnp.float32)
        .astype(jnp.bfloat16)
        .reshape(sp_count, slot_cap, D)
    )
    arrived = lax.all_to_all(outbound, "sp", split_axis=0, concat_axis=0, tiled=True)
    item_count = arrived.shape[1]
    flat_rows = arrived.reshape(sp_count * item_count, D)
    row_block = lax.all_gather(flat_rows, "tp", axis=0, tiled=True)
    gate_pre = jnp.dot(row_block, expert_gate[0], preferred_element_type=jnp.float32)
    up_pre = jnp.dot(row_block, expert_up[0], preferred_element_type=jnp.float32)
    hidden = (jax.nn.silu(gate_pre) * up_pre).astype(jnp.bfloat16)
    served = lax.psum_scatter(
        jnp.dot(hidden, expert_down[0], preferred_element_type=jnp.float32).astype(jnp.bfloat16),
        "tp",
        scatter_dimension=0,
        tiled=True,
    ).reshape(sp_count, item_count, D)
    returned_rows = lax.all_to_all(served, "sp", split_axis=0, concat_axis=0, tiled=True).reshape(
        slot_total, D
    )
    picked = (
        jnp.take(returned_rows, targets.reshape(-1), axis=0)
        .reshape(tok_count, TOPK, D)
        .astype(jnp.float32)
    )
    moe_sum = jnp.sum(picked * route_weights[:, :, None], axis=1)
    return (middle + moe_sum).astype(jnp.bfloat16)


def solution(mesh):
    return jax.shard_map(
        shards,
        mesh=mesh,
        in_specs=(
            P("sp", "tp"),
            P("sp", None),
            P("sp", None),
            P(),
            P(None, "tp"),
            P(None, "tp"),
            P(),
            P(),
            P(),
            P(),
            P(("sp", "tp"), None),
            P(),
            P(("sp", "tp"), None),
            P(("sp", "tp"), None),
            P("sp", None, "tp"),
            P("sp", None, "tp"),
            P("sp", "tp", None),
        ),
        out_specs=P(("sp", "tp"), None),
        check_vma=False,
    )
```

profile of v0, /device:TPU:0, one launch (start us, length us, event | category | flops | bytes accessed | tf_op | source)
XLA Modules:
  0.0 237.7 jit_solution(2543511276037347893)
XLA Ops:
  6.6 1.3 fusion.25
  8.0 1.5 bitcast_convert_fusion
  9.5 0.8 broadcast_in_dim.40
  10.6 0.4 convolution_convert_fusion.3
  11.3 0.8 pad_maximum_fusion.1
  13.1 0.7 maximum_bitcast_fusion.1
  13.8 29.8 %all-gather.3.cloned.1.call-done = bf16[2,160,2048]{2,1,0:T(8,128)(2,1)} async-done(((bf16[2,160,512]{2,1,0:T(8,128)(2,1)}), bf16[2,160,2048]{2,1,0:T(8,128)(2,1)}) %all-gather.3.cloned.1.call-update) | async-done | bytes 1310736 | tf_op jit(solution)/shard_map/all_gather | solution.py:118
  43.6 0.7 broadcast_in_dim.39
  44.3 5.1 %while.18 = (s32[]{:T(128)}, f32[2,512]{1,0:T(2,128)S(1)}, f32[2,512]{1,0:T(2,128)S(1)}, f32[2,512,64]{1,2,0:T(8,128)}, s32[]{:T(128)}, /*index=5*/bf16[2,160,20...) while((s32[]{:T(128)}, f32[2,512]{1,0:T(2,128)S(1)}, ...), condition=%wide.region_8.9_spmd.clone, body=%wide.region_3.8_spmd.clone.sunk | while | flops 174984192 | bytes 8466765 | solution.py:153
  44.3 5.0 %conditional.3 = ((f32[2,512]{1,0:T(2,128)S(1)}, f32[2,512]{1,0:T(2,128)S(1)}, f32[2,512,64]{1,2,0:T(8,128)})) conditional(s32[]{:T(128)} %convert_element_type.181, (f32[2,512]{1,0:T(2,128)S(1)}, f32[2,512]{1,0:T(2,128)S(1)}, f32[2,512,64]{1,2,0:T(8,128)}) %tuple.52, (s32[]{:T(128)}, s32[]{:T(128)}, s32[]{:T(128)}, bf16[2,160,2048]{2,1,0:T(8,128)(2,1)}, ...), branch_computations={%region_4.0_spmd, %region_5.7_spmd} | conditional | flops 174984192 | bytes 8464494 | solution.py:151
  44.6 1.7 fusion.2
  46.3 0.6 fusion.4
  46.8 2.5 %convolution_add_fusion = f32[2,512,64]{1,2,0:T(8,128)} fusion(f32[2,512,512]{2,1,0:T(8,128)S(1)} %get-tuple-element.232, f32[2,512]{1,0:T(2,128)S(1)} %max.2, pred[512,512]{0,1:T(8,128)(4,1)S(1)} %broadcast_compare_fusion, f32[2,512,64]{1,2,0:T(8,128)} %get-tuple-element.169, bf16[2,160,2048]{2,1,0:T(8,128)(2,1)} %get-tuple-element.165, s32[]{:T(128)S(6)} %add.179, ...), kind=kOutput, calls=%fused_computation.7 | convolution fusion | flops 69861376 | bytes 3022856 | tf_op jit(solution)/shard_map/while/body/eval_jaxpr/cond/branch_1_fun/hqk,hvk->hqv/dot_general | solution.py:143
  49.4 1.0 fusion.47
  50.6 0.8 copy.46
  51.5 4.6 %all-to-all-start = ((bf16[8,64,128]{2,1,0:T(8,128)(2,1)}), bf16[8,64,128]{2,1,0:T(8,128)(2,1)S(1)}, u32[]{:S(2)}, u32[]{:S(2)}) async-start(bf16[8,64,128]{2,1,0:T(8,128)(2,1)} %copy.46), calls=%async_computation | async-start | bytes 262144 | tf_op jit(solution)/shard_map/all_to_all | solution.py:157
  56.2 6.6 %all-to-all-done = bf16[8,64,128]{2,1,0:T(8,128)(2,1)S(1)} async-done(((bf16[8,64,128]{2,1,0:T(8,128)(2,1)}), bf16[8,64,128]{2,1,0:T(8,128)(2,1)S(1)}, u32[]{:S(2)}, u32[]{:S(2)}) %all-to-all-start) | async-done | bytes 131104 | tf_op jit(solution)/shard_map/all_to_all | solution.py:157
  62.9 3.0 %fusion.18 = bf16[64,8,2048]{2,0,1:T(8,128)(2,1)S(1)} fusion(bf16[8,128,2048]{2,1,0:T(8,128)(2,1)} %bitcast.57, bf16[8,64,128]{2,1,0:T(8,128)(2,1)S(1)} %all-to-all-done, f32[8,128]{1,0:T(8,128)S(1)} %bitcast.61, f32[64]{0:T(128)S(1)} %add_rsqrt_fusion.4), kind=kOutput, calls=%fused_computation.29 | convolution fusion | flops 269746176 | bytes 6426880 | tf_op jit(solution)/shard_map/tgc,gcd->tgd/dot_general | solution.py:161
  66.3 0.6 copy-done.1
  67.1 0.4 convolution_convert_fusion.2
  67.6 27.1 %all_to_all.23 = bf16[4,36,2048]{2,1,0:T(8,128)(2,1)S(1)} all-to-all(bf16[4,36,2048]{2,1,0:T(8,128)(2,1)S(1)} %reshape.251), channel_id=1, replica_groups=mesh['sp'=4,'tp'=8] {'sp'}, dimensions={0} | all-to-all | bytes 1179648 | tf_op jit(solution)/shard_map/all_to_all | solution.py:180
  94.7 1.0 reshape.252
  95.9 48.8 %all-gather.5.cloned.1.call-done = bf16[1152,2048]{1,0:T(8,128)(2,1)} async-done(((bf16[144,2048]{1,0:T(8,128)(2,1)}), bf16[1152,2048]{1,0:T(8,128)(2,1)}) %all-gather.5.cloned.1.call-update) | async-done | bytes 4718608 | tf_op jit(solution)/shard_map/all_gather | solution.py:183
  144.7 5.0 %fusion.31 = f32[1152,256]{1,0:T(8,128)} fusion(bf16[1152,2048]{1,0:T(8,128)(2,1)} %all-gather.5.cloned.1.call-done, bf16[1,2048,256]{2,1,0:T(8,128)(2,1)} %param.35), kind=kOutput, calls=%fused_computation.46 | convolution fusion | flops 1207959552 | bytes 6946816 | tf_op jit(solution)/shard_map/dot_general | solution.py:184
  149.7 9.7 %convolution_convert_fusion = bf16[1152,2048]{1,0:T(8,128)(2,1)} fusion(bf16[1152,2048]{1,0:T(8,128)(2,1)} %all-gather.5.cloned.1.call-done, f32[1152,256]{1,0:T(8,128)} %fusion.31, bf16[1,256,2048]{2,1,0:T(8,128)(2,1)S(1)} %copy-done, bf16[1,2048,256]{2,1,0:T(8,128)(2,1)S(1)} %copy-done.10), kind=kOutput, calls=%fused_computation.25 | convolution fusion | flops 2420047872 | bytes 12713984 | tf_op jit(solution)/shard_map/dot_general | solution.py:188
  159.5 53.8 %reduce-scatter.2.cloned.1.call-done = bf16[144,2048]{1,0:T(8,128)(2,1)} async-done(((bf16[1152,2048]{1,0:T(8,128)(2,1)}), bf16[144,2048]{1,0:T(8,128)(2,1)}) %reduce-scatter.2.cloned.1.call-update) | async-done | bytes 589840 | tf_op jit(solution)/shard_map/reduce_scatter | solution.py:187
  213.3 2.0 reshape.253
  215.3 3.6 %all-to-all-start.2 = ((bf16[4,36,2048]{2,1,0:T(8,128)(2,1)}), bf16[4,36,2048]{2,1,0:T(8,128)(2,1)S(1)}, u32[]{:S(2)}, u32[]{:S(2)}) async-start(bf16[4,36,2048]{2,1,0:T(8,128)(2,1)} %reshape.253), calls=%async_computation.3 | async-start | bytes 1310720 | tf_op jit(solution)/shard_map/all_to_all | solution.py:193
  219.4 7.2 %all-to-all-done.2 = bf16[4,36,2048]{2,1,0:T(8,128)(2,1)S(1)} async-done(((bf16[4,36,2048]{2,1,0:T(8,128)(2,1)}), bf16[4,36,2048]{2,1,0:T(8,128)(2,1)S(1)}, u32[]{:S(2)}, u32[]{:S(2)}) %all-to-all-start.2) | async-done | bytes 589856 | tf_op jit(solution)/shard_map/all_to_all | solution.py:193
  226.7 0.9 gather_fusion
  228.0 2.3 multiply_reduce_fusion
  230.4 0.8 add_convert_fusion
  (83 shorter events, 4.1 us)
Async XLA Ops:
  6.5 143.2 %copy-start = (bf16[1,256,2048]{2,1,0:T(8,128)(2,1)S(1)}, bf16[1,256,2048]{2,1,0:T(8,128)(2,1)}, u32[]{:S(2)}) copy-start(bf16[1,256,2048]{2,1,0:T(8,128)(2,1)} %param.37) | copy-start | bytes 3145732
  6.5 4.1 %copy-start.3 = (bf16[512,512]{1,0:T(8,128)(2,1)S(1)}, bf16[512,512]{1,0:T(8,128)(2,1)}, u32[]{:S(2)}) copy-start(bf16[512,512]{1,0:T(8,128)(2,1)} %param.22) | copy-start | bytes 1572868
  6.5 4.1 %copy-start.12 = (f32[512]{0:T(512)S(1)}, f32[512]{0:T(512)}, u32[]{:S(2)}) copy-start(f32[512]{0:T(512)} %param.24) | copy-start | bytes 6148
  6.5 3.8 %copy-start.2 = (bf16[512,192]{0,1:T(8,128)(2,1)S(1)}, bf16[512,192]{0,1:T(8,128)(2,1)}, u32[]{:S(2)}) copy-start(bf16[512,192]{0,1:T(8,128)(2,1)} %param.21) | copy-start | bytes 589828
  6.5 3.9 %copy-start.8 = (f32[96]{0:T(128)S(1)}, f32[96]{0:T(128)}, u32[]{:S(2)}) copy-start(f32[96]{0:T(128)} %param.27) | copy-start | bytes 1156
  6.5 3.9 %copy-start.9 = (f32[96]{0:T(128)S(1)}, f32[96]{0:T(128)}, u32[]{:S(2)}) copy-start(f32[96]{0:T(128)} %param.28) | copy-start | bytes 1156
  6.6 4.1 %copy-start.11 = (bf16[512,128]{1,0:T(8,128)(2,1)S(1)}, bf16[512,128]{1,0:T(8,128)(2,1)}, u32[]{:S(2)}) copy-start(bf16[512,128]{1,0:T(8,128)(2,1)} %param.26) | copy-start | bytes 393220
  6.6 37.0 %all-gather.3.cloned.1.call-start = ((), (), s32[]{:S(2)}) async-start(), calls=%async_computation.4 | async-start | bytes 1638400 | tf_op jit(solution)/shard_map/all_gather | solution.py:118
  10.5 1.7 copy-start.4
  44.3 18.6 %copy-start.6 = (f32[1024]{0:T(1024)S(1)}, f32[1024]{0:T(1024)}, u32[]{:S(2)}) copy-start(f32[1024]{0:T(1024)} %param.29) | copy-start | bytes 12292
  51.5 11.3 %all-to-all-start = ((bf16[8,64,128]{2,1,0:T(8,128)(2,1)}), bf16[8,64,128]{2,1,0:T(8,128)(2,1)S(1)}, u32[]{:S(2)}, u32[]{:S(2)}) async-start(bf16[8,64,128]{2,1,0:T(8,128)(2,1)} %copy.46), calls=%async_computation | async-start | bytes 262144 | tf_op jit(solution)/shard_map/all_to_all | solution.py:157
  56.1 88.6 %all-gather.5.cloned.1.call-start = ((), (), s32[]{:S(2)}) async-start(), calls=%async_computation.5 | async-start | bytes 5308416 | tf_op jit(solution)/shard_map/all_gather | solution.py:183
  65.9 1.0 copy-start.1
  65.9 1.1 copy-start.5
  95.6 54.1 %copy-start.10 = (bf16[1,2048,256]{2,1,0:T(8,128)(2,1)S(1)}, bf16[1,2048,256]{2,1,0:T(8,128)(2,1)}, u32[]{:S(2)}) copy-start(bf16[1,2048,256]{2,1,0:T(8,128)(2,1)} %param.36) | copy-start | bytes 3145732
  95.7 117.6 %reduce-scatter.2.cloned.1.call-start = ((), (), s32[]{:S(2)}) async-start(), calls=%async_computation.6 | async-start | bytes 5308416 | tf_op jit(solution)/shard_map/reduce_scatter | solution.py:187
  159.5 59.8 %copy-start.7 = (f32[64,2]{0,1:T(2,128)S(1)}, f32[64,2]{0,1:T(2,128)}, u32[]{:S(2)}) copy-start(f32[64,2]{0,1:T(2,128)} %param.34) | copy-start | bytes 1540
  215.3 11.3 %all-to-all-start.2 = ((bf16[4,36,2048]{2,1,0:T(8,128)(2,1)}), bf16[4,36,2048]{2,1,0:T(8,128)(2,1)S(1)}, u32[]{:S(2)}, u32[]{:S(2)}) async-start(bf16[4,36,2048]{2,1,0:T(8,128)(2,1)} %reshape.253), calls=%async_computation.3 | async-start | bytes 1310720 | tf_op jit(solution)/shard_map/all_to_all | solution.py:193
Sparse Core Ops, SparseCore 0:
  12.3 31.2 all-gather.2
  95.8 48.8 all-gather.4
  159.6 53.6 reduce-scatter.1
where the time goes:
time: 238 us
  waiting for transfers between devices  146 us (61%)
  blocking collectives  27.1 us (11%)
  matrix products  24.2 us (10%)
  between operations  13.5 us (6%)
  other arithmetic  9.45 us (4%)
  local copies, waits for them, and re-layouts  8.58 us (4%)
  starting transfers between devices  8.54 us (4%)
    reduce_scatter x1, waiting for transfers between devices, shards(): lax.psum_scatter(jnp.dot(hidden, expert_down[0], preferred_element_type=j...  53.8 us
    all_gather x1, waiting for transfers between devices, shards(): row_block = lax.all_gather(flat_rows, 'tp', axis=0, tiled=True)  48.8 us
    all_gather x1, waiting for transfers between devices, shards(): key_piece = lax.all_gather(bundle, 'sp', axis=2, tiled=True)  29.8 us
    all_to_all x1, blocking collectives, shards(): lax.all_to_all(outbound, 'sp', split_axis=0, concat_axis=0, tiled=True)  27.1 us
    dot_general x1, matrix products, shards(): jnp.dot(hidden, expert_down[0], preferred_element_type=jnp.float32)  9.73 us
    all_to_all x1, waiting for transfers between devices, shards(): lax.all_to_all(served, 'sp', split_axis=0, concat_axis=0, tiled=True)  7.23 us
    all_to_all x1, waiting for transfers between devices, shards(): lax.all_to_all(head_major, 'tp', split_axis=0, concat_axis=1, tiled=True)  6.6 us
    dot_general x1, matrix products, shards(): jnp.dot(row_block, expert_gate[0], preferred_element_type=jnp.float32)  5.04 us
  transfers between devices with their start and end apart: 5, of which 5 were waited for; matrix products, arithmetic and copies ran while one was open for 1% of the time, Pallas kernels for 0%

commit v1 on v0

--- a/solution.py
+++ b/solution.py
@@ -1,6 +1,10 @@
+import functools
+
 import jax
 import jax.numpy as jnp
 from jax import lax
+from jax.experimental import pallas as pl
+from jax.experimental.pallas import tpu as pltpu
 from jax.sharding import PartitionSpec as P
 
 D = 2048
@@ -10,9 +14,299 @@
 TOPK = 2
 QK = 96
 
-
 epsilon = 1e-06
 rope_base = 10000.0
+MESH_ID = pl.DeviceIdType.MESH
+
+
+class Place:
+    def __init__(self, n_sp, n_z):
+        self.n_sp, self.n_z = n_sp, n_z
+        self.sp = lax.axis_index("sp")
+        self.tp = lax.axis_index("tp")
+        self.core = lax.rem(self.tp, 2)
+        self.z = lax.div(self.tp, 2)
+
+    def partner(self):
+        return (self.sp, self.tp + 1 - 2 * self.core)
+
+    def sp_peer(self, step):
+        return lax.rem(self.sp + step, self.n_sp)
+
+    def z_peer(self, step):
+        return lax.rem(self.z + step, self.n_z)
+
+    def sp_id(self, index):
+        return (index, self.tp)
+
+    def z_id(self, index):
+        return (self.sp, 2 * index + self.core)
+
+    def barrier(self, use_sp, use_z):
+        sem = pltpu.get_barrier_semaphore()
+        count = 1
+        pl.semaphore_signal(sem, inc=1, device_id=self.partner(), device_id_type=MESH_ID)
+        if use_sp:
+            for step in range(1, self.n_sp):
+                pl.semaphore_signal(
+                    sem, inc=1, device_id=self.sp_id(self.sp_peer(step)), device_id_type=MESH_ID
+                )
+            count += self.n_sp - 1
+        if use_z:
+            for step in range(1, self.n_z):
+                pl.semaphore_signal(
+                    sem, inc=1, device_id=self.z_id(self.z_peer(step)), device_id_type=MESH_ID
+                )
+            count += self.n_z - 1
+        pl.semaphore_wait(sem, count)
+
+
+def remote(src, dst, send, recv, device):
+    return pltpu.make_async_remote_copy(
+        src_ref=src,
+        dst_ref=dst,
+        send_sem=send,
+        recv_sem=recv,
+        device_id=device,
+        device_id_type=MESH_ID,
+    )
+
+
+class GroupMove:
+    def __init__(self, place, axis, scatter, x_ref, o_ref, sems):
+        self.place, self.axis, self.scatter = place, axis, scatter
+        self.x_ref, self.o_ref = x_ref, o_ref
+        self.local_sem, self.ss, self.rs, self.ps, self.pr = sems
+        self.count = place.n_sp if axis == "sp" else place.n_z
+        self.me = place.sp if axis == "sp" else place.z
+
+    def start(self):
+        p, core = self.place, self.place.core
+        peer, to_id = (p.sp_peer, p.sp_id) if self.axis == "sp" else (p.z_peer, p.z_id)
+        own = self.x_ref.at[self.me] if self.scatter else self.x_ref
+        self.copies = []
+        for step in range(1, self.count):
+            dst = peer(step)
+            src = self.x_ref.at[dst] if self.scatter else self.x_ref
+            copy = remote(
+                src,
+                self.o_ref.at[core, self.me],
+                self.ss.at[step],
+                self.rs.at[step],
+                to_id(dst),
+            )
+            copy.start()
+            self.copies.append(copy)
+        self.local = pltpu.make_async_copy(own, self.o_ref.at[core, self.me], self.local_sem.at[0])
+        self.local.start()
+        self.relays = [
+            remote(
+                own, self.o_ref.at[core, self.me], self.ps.at[0], self.pr.at[0], p.partner()
+            )
+        ]
+        self.relays[0].start()
+
+    def relay(self):
+        core = self.place.core
+        for step in range(1, self.count):
+            src = lax.rem(self.me - step + self.count, self.count)
+            self.copies[step - 1].wait_recv()
+            block = self.o_ref.at[core, src]
+            copy = remote(block, block, self.ps.at[step], self.pr.at[step], self.place.partner())
+            copy.start()
+            self.relays.append(copy)
+
+    def finish(self):
+        for copy in self.copies:
+            copy.wait_send()
+        for copy in self.relays:
+            copy.wait()
+        self.local.wait()
+
+
+def move_sems(count):
+    return [pltpu.SemaphoreType.DMA((1,))] + [pltpu.SemaphoreType.DMA((count,))] * 4
+
+
+def vmem():
+    return pl.BlockSpec(memory_space=pltpu.VMEM)
+
+
+def group_move(x, axis, scatter, n_sp, n_z, collective_id, name):
+    count = n_sp if axis == "sp" else n_z
+    block = x.shape[1:] if scatter else x.shape
+
+    def kernel(x_ref, o_ref, *sems):
+        place = Place(n_sp, n_z)
+        place.barrier(axis == "sp", axis == "z")
+        move = GroupMove(place, axis, scatter, x_ref, o_ref, sems)
+        move.start()
+        move.relay()
+        move.finish()
+
+    return pl.pallas_call(
+        kernel,
+        out_shape=jax.ShapeDtypeStruct((2, count) + block, x.dtype),
+        in_specs=[vmem()],
+        out_specs=vmem(),
+        scratch_shapes=move_sems(count),
+        compiler_params=pltpu.CompilerParams(
+            collective_id=collective_id, has_side_effects=True, vmem_limit_bytes=60 << 20
+        ),
+        name=name,
+    )(x)
+
+
+def first_exchange(bundle, residual, meta, n_sp, n_z):
+    def kernel(kv_ref, res_ref, meta_ref, kv_out, res_out, meta_out, kv_local, kv_s, kv_r, *sems):
+        place = Place(n_sp, n_z)
+        place.barrier(True, True)
+        copies = []
+        for step in range(1, n_sp):
+            copy = remote(
+                kv_ref,
+                kv_out.at[place.sp],
+                kv_s.at[step],
+                kv_r.at[step],
+                place.sp_id(place.sp_peer(step)),
+            )
+            copy.start()
+            copies.append(copy)
+        local = pltpu.make_async_copy(kv_ref, kv_out.at[place.sp], kv_local.at[0])
+        local.start()
+        meta_move = GroupMove(place, "z", False, meta_ref, meta_out, sems[:5])
+        res_move = GroupMove(place, "z", False, res_ref, res_out, sems[5:])
+        meta_move.start()
+        res_move.start()
+        meta_move.relay()
+        res_move.relay()
+        for copy in copies:
+            copy.wait()
+        local.wait()
+        meta_move.finish()
+        res_move.finish()
+
+    return pl.pallas_call(
+        kernel,
+        out_shape=(
+            jax.ShapeDtypeStruct((n_sp,) + bundle.shape, bundle.dtype),
+            jax.ShapeDtypeStruct((2, n_z) + residual.shape, residual.dtype),
+            jax.ShapeDtypeStruct((2, n_z) + meta.shape, meta.dtype),
+        ),
+        in_specs=[vmem()] * 3,
+        out_specs=(vmem(),) * 3,
+        scratch_shapes=[
+            pltpu.SemaphoreType.DMA((1,)),
+            pltpu.SemaphoreType.DMA((n_sp,)),
+            pltpu.SemaphoreType.DMA((n_sp,)),
+        ]
+        + move_sems(n_z) * 2,
+        compiler_params=pltpu.CompilerParams(
+            collective_id=0, has_side_effects=True, vmem_limit_bytes=60 << 20
+        ),
+        name="first_exchange",
+    )(bundle, residual, meta)
+
+
+CHUNKS = 4
+
+
+def return_rows(partial, mixer, middle, n_sp, n_z):
+    rows = partial.shape[2]
+    tok = middle.shape[0]
+    width = D // CHUNKS
+
+    def kernel(y_ref, mix_ref, mid_ref, o_ref, pbuf, sbuf, rbuf, cbuf, fbuf, *sems):
+        pair_s, pair_r, sp_s, sp_r, z_s, z_r = sems
+        place = Place(n_sp, n_z)
+        core = place.core
+        place.barrier(True, True)
+        pairs, sends, zsends = {}, {}, {}
+        order = list(range(1, n_sp)) + [0]
+        for q in range(CHUNKS):
+            cols = pl.ds(q * width, width)
+            for step in order:
+                dst = place.sp_peer(step)
+                copy = remote(
+                    y_ref.at[1 - core, dst, :, cols],
+                    pbuf.at[dst, :, cols],
+                    pair_s.at[q, step],
+                    pair_r.at[q, step],
+                    place.partner(),
+                )
+                copy.start()
+                pairs[q, step] = copy
+        for q in range(CHUNKS):
+            cols = pl.ds(q * width, width)
+            for step in order:
+                dst = place.sp_peer(step)
+                pairs[q, step].wait_recv()
+                total = (
+                    y_ref[core, dst, :, cols].astype(jnp.float32)
+                    + pbuf[dst, :, cols].astype(jnp.float32)
+                ).astype(jnp.bfloat16)
+                if step == 0:
+                    rbuf[dst, :, cols] = total
+                else:
+                    sbuf[dst, :, cols] = total
+                    copy = remote(
+                        sbuf.at[dst, :, cols],
+                        rbuf.at[place.sp, :, cols],
+                        sp_s.at[q, step],
+                        sp_r.at[q, step],
+                        place.sp_id(dst),
+                    )
+                    copy.start()
+                    sends[q, step] = copy
+        for q in range(CHUNKS):
+            cols = pl.ds(q * width, width)
+            for step in range(1, n_sp):
+                sends[q, step].wait_recv()
+            combined = jnp.zeros((n_z * tok, width), jnp.float32)
+            for src in range(n_sp):
+                combined += jnp.dot(
+                    mix_ref[src], rbuf[src, :, cols], preferred_element_type=jnp.float32
+                )
+            cbuf[:, :, cols] = combined.astype(jnp.bfloat16).reshape(n_z, tok, width)
+            for step in range(1, n_z):
+                dst = place.z_peer(step)
+                copy = remote(
+                    cbuf.at[dst, :, cols],
+                    fbuf.at[place.z, :, cols],
+                    z_s.at[q, step],
+                    z_r.at[q, step],
+                    place.z_id(dst),
+                )
+                copy.start()
+                zsends[q, step] = copy
+        for q in range(CHUNKS):
+            cols = pl.ds(q * width, width)
+            total = mid_ref[:, cols] + cbuf[place.z, :, cols].astype(jnp.float32)
+            for step in range(1, n_z):
+                src = lax.rem(place.z - step + n_z, n_z)
+                zsends[q, step].wait_recv()
+                total += fbuf[src, :, cols].astype(jnp.float32)
+            o_ref[:, cols] = total.astype(jnp.bfloat16)
+        for group in (pairs, sends, zsends):
+            for copy in group.values():
+                copy.wait_send()
+
+    dma = pltpu.SemaphoreType.DMA
+    block = pltpu.VMEM((n_sp, rows, D), jnp.bfloat16)
+    zblock = pltpu.VMEM((n_z, tok, D), jnp.bfloat16)
+    return pl.pallas_call(
+        kernel,
+        out_shape=jax.ShapeDtypeStruct((tok, D), jnp.bfloat16),
+        in_specs=[vmem()] * 3,
+        out_specs=vmem(),
+        scratch_shapes=[block, block, block, zblock, zblock]
+        + [dma((CHUNKS, n_sp))] * 4
+        + [dma((CHUNKS, n_z))] * 2,
+        compiler_params=pltpu.CompilerParams(
+            collective_id=3, has_side_effects=True, vmem_limit_bytes=60 << 20
+        ),
+        name="return_rows",
+    )(partial, mixer, middle)
 
 
 def rms_scale(values):
@@ -38,21 +332,6 @@
     normed_rows = raw_rows * rms_scale(raw_rows) * gain_vec
     turned_rows = rotate_half(normed_rows[..., NOPE:], angles[:, None, :])
     return jnp.concatenate([normed_rows[..., :NOPE], turned_rows], axis=-1).astype(jnp.bfloat16)
-
-
-def slot_targets(route_rows, expert_total, slot_cap):
-    flat_routes = route_rows.reshape(-1)
-    one_hot = (flat_routes[:, None] == jnp.arange(expert_total, dtype=jnp.int32)[None, :]).astype(
-        jnp.int32
-    )
-    earlier = jnp.cumsum(one_hot, axis=0) - one_hot
-    rank_in = jnp.sum(earlier * one_hot, axis=1)
-    return (flat_routes * slot_cap + rank_in).reshape(route_rows.shape)
-
-
-def select_matrix(targets, slot_total):
-    hits = targets[:, :, None] == jnp.arange(slot_total, dtype=jnp.int32)[None, None, :]
-    return jnp.sum(hits.astype(jnp.bfloat16), axis=1)
 
 
 def shards(
@@ -78,6 +357,8 @@
     local_heads = key_up.shape[1] // NOPE
     sp_count = lax.axis_size("sp")
     tp_count = lax.axis_size("tp")
+    z_count = tp_count // 2
+    tok_count = residual.shape[0]
     my_first = lax.axis_index("sp") * shard_len
     my_last = my_first + shard_len - 1
     positions = my_first + jnp.arange(shard_len, dtype=jnp.int32)
@@ -115,15 +396,23 @@
         jnp.zeros((local_heads, shard_len), jnp.float32),
         jnp.zeros((local_heads, shard_len, VH), jnp.float32),
     )
-    key_piece = lax.all_gather(bundle, "sp", axis=2, tiled=True)
-    block_count = key_piece.shape[2] // shard_len
+    meta = jnp.concatenate(
+        [
+            routes.astype(jnp.float32),
+            route_weights,
+            jnp.zeros((tok_count, 128 - 2 * TOPK), jnp.float32),
+        ],
+        axis=1,
+    )
+    key_piece, residual_all, meta_all = first_exchange(bundle, residual, meta, sp_count, z_count)
+    block_count = sp_count
 
     def one_block(block_index, running_state):
         first_key = block_index * shard_len
 
         def compute(inner):
             row_peak, row_total, weighted = inner
-            key_part = lax.dynamic_slice_in_dim(key_piece, block_index * shard_len, shard_len, 2)
+            key_part = lax.dynamic_index_in_dim(key_piece, block_index, 0, keepdims=False)
             scores = (
                 jnp.einsum(
                     "hqc,hck->hqk",
@@ -152,54 +441,53 @@
 
     row_peak, row_total, weighted = lax.fori_loop(0, block_count, one_block, init_state)
     attended = (weighted / row_total[..., None]).astype(jnp.bfloat16)
-    tok_count = residual.shape[0]
     head_major = jnp.transpose(attended, (1, 0, 2)).reshape(shard_len, local_heads * VH)
-    token_rows = lax.all_to_all(head_major, "tp", split_axis=0, concat_axis=1, tiled=True).astype(
-        jnp.float32
-    )
-    normed_rows = (token_rows * rms_scale(token_rows) * out_gain).astype(jnp.bfloat16)
-    partials = jnp.einsum(
-        "tgc,gcd->tgd",
-        normed_rows.reshape(tok_count, tp_count, -1),
-        out_weight.reshape(tp_count, -1, D),
-        preferred_element_type=jnp.float32,
-    )
-    rounded = lax.optimization_barrier(partials.astype(jnp.bfloat16))
-    mixed = jnp.sum(rounded.astype(jnp.float32), axis=1)
-    middle = residual.astype(jnp.float32) + mixed
+    gathered = group_move(head_major, "z", False, sp_count, z_count, 1, "gather_heads")
+    att_rows = (
+        jnp.transpose(gathered, (2, 1, 0, 3)).reshape(shard_len, -1).astype(jnp.float32)
+    )
+    normed_rows = (att_rows * rms_scale(att_rows) * out_gain).astype(jnp.bfloat16)
+    mixed = jnp.dot(normed_rows, out_weight, preferred_element_type=jnp.float32)
+    residual_rows = jnp.transpose(residual_all, (1, 0, 2, 3)).reshape(shard_len, D)
+    middle = residual_rows.astype(jnp.float32) + mixed
     ffn_input = (middle * rms_scale(middle) * ffn_gain).astype(jnp.bfloat16)
+    own_middle = lax.dynamic_slice_in_dim(
+        middle, lax.axis_index("tp") * tok_count, tok_count, 0
+    )
     slot_cap = max(2, 9 * tok_count * TOPK // (8 * sp_count))
-    slot_total = sp_count * slot_cap
-    targets = slot_targets(routes, sp_count, slot_cap)
-    chooser = select_matrix(targets, slot_total)
+    rows = z_count * slot_cap
+    core = lax.axis_index("tp") % 2
+    part_meta = lax.dynamic_index_in_dim(meta_all, core, 0, keepdims=False)
+    part_routes = part_meta[:, :, :TOPK].astype(jnp.int32).reshape(z_count, tok_count * TOPK)
+    part_weights = part_meta[:, :, TOPK : 2 * TOPK].reshape(z_count * tok_count, TOPK)
+    one_hot = (part_routes[:, :, None] == jnp.arange(sp_count, dtype=jnp.int32)).astype(jnp.int32)
+    earlier = jnp.cumsum(one_hot, axis=1) - one_hot
+    rank_in = jnp.sum(earlier * one_hot, axis=2)
+    slots = rank_in + jnp.arange(z_count, dtype=jnp.int32)[:, None] * slot_cap
+    targets = (part_routes * rows + slots).reshape(z_count * tok_count, TOPK)
+    hits = targets[:, :, None] == jnp.arange(sp_count * rows, dtype=jnp.int32)
+    chooser = jnp.sum(hits.astype(jnp.bfloat16), axis=1)
+    mixer = jnp.sum(jnp.where(hits, part_weights[:, :, None], 0.0), axis=1).astype(jnp.bfloat16)
+    mixer = jnp.transpose(mixer.reshape(z_count * tok_count, sp_count, rows), (1, 0, 2))
+    part_input = lax.dynamic_index_in_dim(
+        ffn_input.reshape(z_count, 2, tok_count, D), core, 1, keepdims=False
+    ).reshape(z_count * tok_count, D)
     outbound = (
-        jnp.einsum("ts,td->sd", chooser, ffn_input, preferred_element_type=jnp.float32)
+        jnp.einsum("ts,td->sd", chooser, part_input, preferred_element_type=jnp.float32)
         .astype(jnp.bfloat16)
-        .reshape(sp_count, slot_cap, D)
-    )
-    arrived = lax.all_to_all(outbound, "sp", split_axis=0, concat_axis=0, tiled=True)
-    item_count = arrived.shape[1]
-    flat_rows = arrived.reshape(sp_count * item_count, D)
-    row_block = lax.all_gather(flat_rows, "tp", axis=0, tiled=True)
+        .reshape(sp_count, rows, D)
+    )
+    arrived = group_move(outbound, "sp", True, sp_count, z_count, 2, "send_rows")
+    row_block = arrived.reshape(2 * sp_count * rows, D)
     gate_pre = jnp.dot(row_block, expert_gate[0], preferred_element_type=jnp.float32)
     up_pre = jnp.dot(row_block, expert_up[0], preferred_element_type=jnp.float32)
     hidden = (jax.nn.silu(gate_pre) * up_pre).astype(jnp.bfloat16)
-    served = lax.psum_scatter(
-        jnp.dot(hidden, expert_down[0], preferred_element_type=jnp.float32).astype(jnp.bfloat16),
-        "tp",
-        scatter_dimension=0,
-        tiled=True,
-    ).reshape(sp_count, item_count, D)
-    returned_rows = lax.all_to_all(served, "sp", split_axis=0, concat_axis=0, tiled=True).reshape(
-        slot_total, D
-    )
-    picked = (
-        jnp.take(returned_rows, targets.reshape(-1), axis=0)
-        .reshape(tok_count, TOPK, D)
-        .astype(jnp.float32)
-    )
-    moe_sum = jnp.sum(picked * route_weights[:, :, None], axis=1)
-    return (middle + moe_sum).astype(jnp.bfloat16)
+    served = jnp.dot(hidden, expert_down[0], preferred_element_type=jnp.float32).astype(
+        jnp.bfloat16
+    )
+    return return_rows(
+        served.reshape(2, sp_count, rows, D), mixer, own_middle, sp_count, z_count
+    )
 
 
 def solution(mesh):

time: 238 us -> 190 us (0.80)
  waiting for transfers between devices: 146 us -> 0 us
  Pallas kernels: 0 us -> 139 us
  blocking collectives: 27.1 us -> 0 us
  between operations: 13.5 us -> 0.4 us
  starting transfers between devices: 8.54 us -> 0 us
  local copies, waits for them, and re-layouts: 8.58 us -> 13.7 us
  other arithmetic: 9.45 us -> 12.6 us
    pallas_call x0 -> x4, Pallas kernels: none -> 139 us  [the longest x2 61.7 us: group_move(): pl.pallas_call(kernel, out_shape=jax.ShapeDtypeStruct((2, count) + block,...]
    all_gather x2 -> x0, waiting for transfers between devices: 78.6 us -> none  [the longest x1 48.8 us: shards(): row_block = lax.all_gather(flat_rows, 'tp', axis=0, tiled=True)]
    reduce_scatter x1 -> x0, waiting for transfers between devices: 53.8 us -> none  [shards(): lax.psum_scatter(jnp.dot(hidden, expert_down[0], preferred_element_type=j...]
    all_to_all x1 -> x0, blocking collectives: 27.1 us -> none  [shards(): lax.all_to_all(outbound, 'sp', split_axis=0, concat_axis=0, tiled=True)]
    all_to_all x2 -> x0, waiting for transfers between devices: 13.8 us -> none  [the longest x1 7.23 us: shards(): lax.all_to_all(served, 'sp', split_axis=0, concat_axis=0, tiled=True)]
    all_to_all x2 -> x0, starting transfers between devices: 8.24 us -> none  [the longest x1 4.6 us: shards(): lax.all_to_all(head_major, 'tp', split_axis=0, concat_axis=1, tiled=True)]
    unnamed x28, local copies, waits for them, and re-layouts: 0.82 us -> 5.5 us
    convert_element_type x0 -> x5, local copies, waits for them, and re-layouts: none -> 4.07 us  [the longest x1 1.94 us: shards(): jnp.transpose(gathered, (2, 1, 0, 3)).reshape(shard_len, -1)]
  transfers between devices with their start and end apart: 5 -> 0, of which waited for: 5 -> 0; matrix products, arithmetic and copies ran while one was open for 1% -> 0% of each run, Pallas kernels for 0% -> 0%
where the time goes in v1:
time: 190 us; the launch traced here: 189 us
  Pallas kernels  139 us (73%)
  matrix products  22.7 us (12%)
  local copies, waits for them, and re-layouts  13.7 us (7%)
  other arithmetic  12.6 us (7%)
    pallas_call x2, Pallas kernels, group_move(): pl.pallas_call(kernel, out_shape=jax.ShapeDtypeStruct((2, count) + block,...  61.7 us
    pallas_call x1, Pallas kernels, return_rows(): pl.pallas_call(kernel, out_shape=jax.ShapeDtypeStruct((tok, D), jnp.bfloa...  45.4 us
    pallas_call x1, Pallas kernels, first_exchange(): pl.pallas_call(kernel, out_shape=(jax.ShapeDtypeStruct((n_sp,) + bundle.s...  32.2 us
    dot_general x1, matrix products, shards(): jnp.dot(hidden, expert_down[0], preferred_element_type=jnp.float32)  9.68 us
    unnamed x28, local copies, waits for them, and re-layouts  5.5 us
    dot_general x1, matrix products, shards(): jnp.dot(row_block, expert_gate[0], preferred_element_type=jnp.float32)  4.82 us
    reduce_sum x4, other arithmetic, rms_scale(): jnp.mean(values * values, axis=-1, keepdims=True) + epsilon  3.82 us

profile of v1, /device:TPU:0, one launch (start us, length us, event | category | flops | bytes accessed | tf_op | source)
XLA Modules:
  0.0 189.0 jit_solution(12383551265906750598)
XLA Ops:
  0.1 0.8 convert_element_type.103
  1.1 1.2 fusion.26
  2.3 1.0 fusion.36
  3.5 0.8 copy.45
  4.3 0.7 maximum_maximum_fusion.meta_ref
  5.2 0.8 broadcast_in_dim.42
  5.9 1.5 convolution_convert_fusion.2
  8.3 0.8 pad_maximum_fusion.1.kv_ref
  9.1 32.2 %first_exchange.1 = (bf16[4,2,160,512]{3,2,1,0:T(8,128)(2,1)S(1)}, bf16[2,4,64,2048]{3,2,1,0:T(8,128)(2,1)}, f32[2,4,64,128]{3,2,1,0:T(8,128)}) custom-call(bf16[2,160,512]{2,1,0:T(8,128)(2,1)} %pad_maximum_fusion.1.kv_ref, bf16[64,2048]{1,0:T(8,128)(2,1)} %res_ref.1, f32[64,128]{1,0:T(8,128)} %maximum_maximum_fusion.meta_ref), custom_call_target="tpu_custom_call" | custom-call | tf_op jit(solution)/shard_map/first_exchange/pallas_call | solution.py:189
  41.3 0.9 dynamic-slice_bitcast_fusion.1
  42.3 2.6 %while.18 = (s32[]{:T(128)}, f32[2,512]{1,0:T(2,128)S(1)}, f32[2,512]{1,0:T(2,128)S(1)}, f32[2,512,64]{1,2,0:T(8,128)S(1)}, s32[]{:T(128)}, /*index=5*/bf16[4,2,...) while((s32[]{:T(128)}, f32[2,512]{1,0:T(2,128)S(1)}, ...), condition=%wide.region_11.12_spmd.clone, body=%wide.region_6.11_spmd.clone.sunk | while | flops 174984192 | bytes 9122101 | solution.py:442
  42.3 2.3 %conditional.3 = ((f32[2,512]{1,0:T(2,128)S(1)}, f32[2,512]{1,0:T(2,128)S(1)}, f32[2,512,64]{1,2,0:T(8,128)S(1)})) conditional(s32[]{:T(128)} %convert_element_type.172, (f32[2,512]{1,0:T(2,128)S(1)}, f32[2,512]{1,0:T(2,128)S(1)}, f32[2,512,64]{1,2,0:T(8,128)S(1)}) %tuple.53, (s32[]{:T(128)}, s32[]{:T(128)}, s32[]{:T(128)}, ...), branch_computations={%region_7.7_spmd, %region_8.10_spmd} | conditional | flops 174984192 | bytes 9119822 | solution.py:440
  42.6 0.6 fusion.2
  43.3 0.6 fusion.4
  43.9 0.8 convolution_add_fusion
  44.9 0.8 copy.50.x_ref
  47.7 1.0 copy.53
  48.9 19.8 %gather_heads.1 = bf16[2,4,512,128]{3,2,1,0:T(8,128)(2,1)} custom-call(bf16[512,128]{1,0:T(8,128)(2,1)} %copy.50.x_ref), custom_call_target="tpu_custom_call" | custom-call | tf_op jit(solution)/shard_map/gather_heads/pallas_call | solution.py:147
  68.7 1.5 fusion.17
  70.2 2.7 %convert_bitcast_fusion.1 = f32[512,4,2,128]{3,0,1,2:T(8,128)} fusion(bf16[2,4,512,128]{3,2,1,0:T(8,128)(2,1)} %gather_heads.1), kind=kLoop, calls=%fused_computation.31 | loop fusion | flops 524288 | bytes 3145728 | tf_op jit(solution)/shard_map/convert_element_type | solution.py:447
  72.9 1.9 %copy.51 = f32[512,4,2,128]{0,3,2,1:T(8,128)S(1)} copy(f32[512,4,2,128]{3,0,1,2:T(8,128)} %convert_bitcast_fusion.1) | data formatting | bytes 4194304 | tf_op jit(solution)/shard_map/convert_element_type | solution.py:447
  75.1 1.3 copy-done.1
  76.5 0.5 convert_bitcast_fusion
  77.5 1.7 copy-done.8
  79.2 2.6 %multiply_reduce_fusion = (f32[512]{0:T(512)S(1)}, f32[512,2048]{1,0:T(8,128)S(1)}) fusion(bf16[512,1024]{0,1:T(8,128)(2,1)S(1)} %fusion.19, bf16[1024,2048]{1,0:T(8,128)(2,1)S(1)} %copy-done.8, f32[4,2,64,2048]{3,2,1,0:T(8,128)S(1)} %copy.49), kind=kOutput, calls=%fused_computation.27 | convolution fusion | flops 2150628864 | bytes 13633536 | tf_op jit(solution)/shard_map/dot_general | solution.py:450
  81.8 0.8 constant_dynamic-slice_fusion.1.mid_ref
  83.2 2.2 %convolution_convert_fusion.1 = bf16[576,2048]{1,0:T(8,128)(2,1)} fusion(bf16[256,576]{0,1:T(8,128)(2,1)S(1)} %fusion.34, bf16[256,2048]{1,0:T(8,128)(2,1)S(1)} %bitcast.77), kind=kOutput, calls=%fused_computation.28 | convolution fusion | flops 605159424 | bytes 3702784 | tf_op jit(solution)/shard_map/ts,td->sd/dot_general | solution.py:476
  85.4 42.0 %send_rows.1 = bf16[2,4,144,2048]{3,2,1,0:T(8,128)(2,1)} custom-call(bf16[4,144,2048]{2,1,0:T(8,128)(2,1)} %bitcast.72), custom_call_target="tpu_custom_call" | custom-call | tf_op jit(solution)/shard_map/send_rows/pallas_call | solution.py:147
  127.4 4.8 %fusion.32 = f32[1152,256]{1,0:T(8,128)} fusion(bf16[1152,2048]{1,0:T(8,128)(2,1)} %bitcast.75, bf16[1,2048,256]{2,1,0:T(8,128)(2,1)S(1)} %copy-done.9), kind=kOutput, calls=%fused_computation.54 | convolution fusion | flops 1207959552 | bytes 6946816 | tf_op jit(solution)/shard_map/dot_general | solution.py:482
  132.2 9.7 %convolution_convert_fusion = bf16[1152,2048]{1,0:T(8,128)(2,1)} fusion(bf16[1152,2048]{1,0:T(8,128)(2,1)} %bitcast.76, f32[1152,256]{1,0:T(8,128)} %fusion.32, bf16[1,256,2048]{2,1,0:T(8,128)(2,1)S(1)} %copy-done, bf16[1,2048,256]{2,1,0:T(8,128)(2,1)S(1)} %copy-done.10), kind=kOutput, calls=%fused_computation.23 | convolution fusion | flops 2420047872 | bytes 12713984 | tf_op jit(solution)/shard_map/dot_general | solution.py:485
  141.9 45.4 %return_rows.1 = bf16[64,2048]{1,0:T(8,128)(2,1)} custom-call(bf16[2,4,144,2048]{3,2,1,0:T(8,128)(2,1)} %bitcast.74, bf16[4,256,144]{2,1,0:T(8,128)(2,1)} %bitcast.78, f32[64,2048]{1,0:T(8,128)} %constant_dynamic-slice_fusion.1.mid_ref), custom_call_target="tpu_custom_call" | custom-call | tf_op jit(solution)/shard_map/return_rows/pallas_call | solution.py:297
  187.3 1.7 copy.75
  (80 shorter events, 5.2 us)
Async XLA Ops:
  0.0 132.2 %copy-start = (bf16[1,256,2048]{2,1,0:T(8,128)(2,1)S(1)}, bf16[1,256,2048]{2,1,0:T(8,128)(2,1)}, u32[]{:S(2)}) copy-start(bf16[1,256,2048]{2,1,0:T(8,128)(2,1)} %param.37) | copy-start | bytes 3145732
  0.0 7.4 %copy-start.3 = (bf16[512,512]{1,0:T(8,128)(2,1)S(1)}, bf16[512,512]{1,0:T(8,128)(2,1)}, u32[]{:S(2)}) copy-start(bf16[512,512]{1,0:T(8,128)(2,1)} %param.22) | copy-start | bytes 1572868
  0.0 7.5 %copy-start.12 = (f32[512]{0:T(512)S(1)}, f32[512]{0:T(512)}, u32[]{:S(2)}) copy-start(f32[512]{0:T(512)} %param.24) | copy-start | bytes 6148
  0.0 8.0 %copy-start.6 = (f32[96]{0:T(128)S(1)}, f32[96]{0:T(128)}, u32[]{:S(2)}) copy-start(f32[96]{0:T(128)} %param.28) | copy-start | bytes 1156
  0.0 7.5 %copy-start.11 = (bf16[512,128]{1,0:T(8,128)(2,1)S(1)}, bf16[512,128]{1,0:T(8,128)(2,1)}, u32[]{:S(2)}) copy-start(bf16[512,128]{1,0:T(8,128)(2,1)} %param.25) | copy-start | bytes 393220
  2.3 5.8 %copy-start.2 = (bf16[512,192]{0,1:T(8,128)(2,1)S(1)}, bf16[512,192]{0,1:T(8,128)(2,1)}, u32[]{:S(2)}) copy-start(bf16[512,192]{0,1:T(8,128)(2,1)} %param.21) | copy-start | bytes 589828
  2.3 5.8 %copy-start.7 = (f32[96]{0:T(128)S(1)}, f32[96]{0:T(128)}, u32[]{:S(2)}) copy-start(f32[96]{0:T(128)} %param.27) | copy-start | bytes 1156
  72.9 2.0 %copy-start.5 = (f32[1024]{0:T(1024)S(1)}, f32[1024]{0:T(1024)}, u32[]{:S(2)}) copy-start(f32[1024]{0:T(1024)} %param.29) | copy-start | bytes 12292
  74.9 1.6 copy-start.1
  77.0 2.2 %copy-start.8 = (bf16[1024,2048]{1,0:T(8,128)(2,1)S(1)}, bf16[1024,2048]{1,0:T(8,128)(2,1)}, u32[]{:S(2)}) copy-start(bf16[1024,2048]{1,0:T(8,128)(2,1)} %param.30) | copy-start | bytes 12582916
  79.2 3.5 %copy-start.4 = (f32[2048]{0:T(1024)S(1)}, f32[2048]{0:T(1024)}, u32[]{:S(2)}) copy-start(f32[2048]{0:T(1024)} %param.32) | copy-start | bytes 24580
  85.4 42.0 %copy-start.9 = (bf16[1,2048,256]{2,1,0:T(8,128)(2,1)S(1)}, bf16[1,2048,256]{2,1,0:T(8,128)(2,1)}, u32[]{:S(2)}) copy-start(bf16[1,2048,256]{2,1,0:T(8,128)(2,1)} %param.35) | copy-start | bytes 3145732
  127.4 4.8 %copy-start.10 = (bf16[1,2048,256]{2,1,0:T(8,128)(2,1)S(1)}, bf16[1,2048,256]{2,1,0:T(8,128)(2,1)}, u32[]{:S(2)}) copy-start(bf16[1,2048,256]{2,1,0:T(8,128)(2,1)} %param.36) | copy-start | bytes 3145732

commit v2 on v1

--- a/solution.py
+++ b/solution.py
@@ -208,15 +208,85 @@
     )(bundle, residual, meta)
 
 
+def send_rows(x, n_sp, n_z):
+    rows, shared = x.shape[1], D // 4
+    half = (D - shared) // 2
+
+    def kernel(x_ref, o_ref, local_sem, *sems):
+        place = Place(n_sp, n_z)
+        core, me = place.core, place.sp
+        place.barrier(True, True)
+        side = lax.rem(place.z, 2)
+        twin = place.z_id(place.z + 1 - 2 * side)
+        mine = pl.ds(pl.multiple_of(shared + side * half, 128), half)
+        other = pl.ds(pl.multiple_of(shared + (1 - side) * half, 128), half)
+        both = pl.ds(0, shared)
+        copies = []
+
+        def push(kind, step, src, dst, device):
+            copy = remote(src, dst, sems[2 * kind].at[step], sems[2 * kind + 1].at[step], device)
+            copy.start()
+            copies.append(copy)
+            return copy
+
+        split, direct, swapped = {}, {}, {}
+        for step in range(1, n_sp):
+            dst = place.sp_peer(step)
+            split[step] = push(
+                0, step, x_ref.at[dst, :, mine], o_ref.at[core, me, :, mine], place.sp_id(dst)
+            )
+        for step in range(1, n_sp):
+            dst = place.sp_peer(step)
+            direct[step] = push(
+                1, step, x_ref.at[dst, :, both], o_ref.at[core, me, :, both], place.sp_id(dst)
+            )
+        local = pltpu.make_async_copy(x_ref.at[me], o_ref.at[core, me], local_sem.at[0])
+        local.start()
+        last = [push(3, 0, x_ref.at[me], o_ref.at[core, me], place.partner())]
+        for step in range(1, n_sp):
+            src = lax.rem(me - step + n_sp, n_sp)
+            piece = o_ref.at[core, src, :, mine]
+            split[step].wait_recv()
+            swapped[step] = push(2, step, piece, piece, twin)
+            last.append(push(3, step, piece, piece, place.partner()))
+        for step in range(1, n_sp):
+            src = lax.rem(me - step + n_sp, n_sp)
+            piece = o_ref.at[core, src, :, both]
+            direct[step].wait_recv()
+            last.append(push(4, step, piece, piece, place.partner()))
+        for step in range(1, n_sp):
+            src = lax.rem(me - step + n_sp, n_sp)
+            piece = o_ref.at[core, src, :, other]
+            swapped[step].wait_recv()
+            last.append(push(5, step, piece, piece, place.partner()))
+        for copy in last:
+            copy.wait_recv()
+        for copy in copies:
+            copy.wait_send()
+        local.wait()
+
+    return pl.pallas_call(
+        kernel,
+        out_shape=jax.ShapeDtypeStruct((2, n_sp, rows, D), x.dtype),
+        in_specs=[vmem()],
+        out_specs=vmem(),
+        scratch_shapes=[pltpu.SemaphoreType.DMA((1,))] + [pltpu.SemaphoreType.DMA((n_sp,))] * 12,
+        compiler_params=pltpu.CompilerParams(
+            collective_id=2, has_side_effects=True, vmem_limit_bytes=60 << 20
+        ),
+        name="send_rows",
+    )(x)
+
+
 CHUNKS = 4
 
 
-def return_rows(partial, mixer, middle, n_sp, n_z):
-    rows = partial.shape[2]
+def return_rows(hidden, down, mixer, middle, n_sp, n_z):
+    rows = hidden.shape[2]
     tok = middle.shape[0]
     width = D // CHUNKS
 
-    def kernel(y_ref, mix_ref, mid_ref, o_ref, pbuf, sbuf, rbuf, cbuf, fbuf, *sems):
+    def kernel(h_ref, w_ref, mix_ref, mid_ref, o_ref, ybuf, pbuf, sbuf, rbuf, cbuf, fbuf, *sems):
         pair_s, pair_r, sp_s, sp_r, z_s, z_r = sems
         place = Place(n_sp, n_z)
         core = place.core
@@ -227,8 +297,11 @@
             cols = pl.ds(q * width, width)
             for step in order:
                 dst = place.sp_peer(step)
+                ybuf[dst, :, cols] = jnp.dot(
+                    h_ref[1 - core, dst], w_ref[:, cols], preferred_element_type=jnp.float32
+                ).astype(jnp.bfloat16)
                 copy = remote(
-                    y_ref.at[1 - core, dst, :, cols],
+                    ybuf.at[dst, :, cols],
                     pbuf.at[dst, :, cols],
                     pair_s.at[q, step],
                     pair_r.at[q, step],
@@ -240,11 +313,11 @@
             cols = pl.ds(q * width, width)
             for step in order:
                 dst = place.sp_peer(step)
+                own = jnp.dot(
+                    h_ref[core, dst], w_ref[:, cols], preferred_element_type=jnp.float32
+                )
                 pairs[q, step].wait_recv()
-                total = (
-                    y_ref[core, dst, :, cols].astype(jnp.float32)
-                    + pbuf[dst, :, cols].astype(jnp.float32)
-                ).astype(jnp.bfloat16)
+                total = (own + pbuf[dst, :, cols].astype(jnp.float32)).astype(jnp.bfloat16)
                 if step == 0:
                     rbuf[dst, :, cols] = total
                 else:
@@ -297,16 +370,16 @@
     return pl.pallas_call(
         kernel,
         out_shape=jax.ShapeDtypeStruct((tok, D), jnp.bfloat16),
-        in_specs=[vmem()] * 3,
+        in_specs=[vmem()] * 4,
         out_specs=vmem(),
-        scratch_shapes=[block, block, block, zblock, zblock]
+        scratch_shapes=[block, block, block, block, zblock, zblock]
         + [dma((CHUNKS, n_sp))] * 4
         + [dma((CHUNKS, n_z))] * 2,
         compiler_params=pltpu.CompilerParams(
             collective_id=3, has_side_effects=True, vmem_limit_bytes=60 << 20
         ),
         name="return_rows",
-    )(partial, mixer, middle)
+    )(hidden, down, mixer, middle)
 
 
 def rms_scale(values):
@@ -477,16 +550,18 @@
         .astype(jnp.bfloat16)
         .reshape(sp_count, rows, D)
     )
-    arrived = group_move(outbound, "sp", True, sp_count, z_count, 2, "send_rows")
+    arrived = send_rows(outbound, sp_count, z_count)
     row_block = arrived.reshape(2 * sp_count * rows, D)
     gate_pre = jnp.dot(row_block, expert_gate[0], preferred_element_type=jnp.float32)
     up_pre = jnp.dot(row_block, expert_up[0], preferred_element_type=jnp.float32)
     hidden = (jax.nn.silu(gate_pre) * up_pre).astype(jnp.bfloat16)
-    served = jnp.dot(hidden, expert_down[0], preferred_element_type=jnp.float32).astype(
-        jnp.bfloat16
-    )
     return return_rows(
-        served.reshape(2, sp_count, rows, D), mixer, own_middle, sp_count, z_count
+        hidden.reshape(2, sp_count, rows, -1),
+        expert_down[0],
+        mixer,
+        own_middle,
+        sp_count,
+        z_count,
     )
 
 

time: 190 us -> 177 us (0.932)
  matrix products: 22.7 us -> 14.5 us
  Pallas kernels: 139 us -> 135 us
    pallas_call x2 -> x1, Pallas kernels: 61.7 us -> 19.8 us  [group_move(): pl.pallas_call(kernel, out_shape=jax.ShapeDtypeStruct((2, count) + block,...]
    pallas_call x0 -> x1, Pallas kernels: none -> 40.2 us  [send_rows(): pl.pallas_call(kernel, out_shape=jax.ShapeDtypeStruct((2, n_sp, rows, D),...]
    dot_general x1, matrix products: 9.68 us -> 2.35 us  [shards(): jnp.dot(row_block, expert_up[0], preferred_element_type=jnp.float32)]
    pallas_call x1, Pallas kernels: 45.4 us -> 43 us  [return_rows(): pl.pallas_call(kernel, out_shape=jax.ShapeDtypeStruct((tok, D), jnp.bfloa...]
where the time goes in v2:
time: 177 us
  Pallas kernels  135 us (76%)
  matrix products  14.5 us (8%)
  local copies, waits for them, and re-layouts  13.8 us (8%)
  other arithmetic  12.6 us (7%)
    pallas_call x1, Pallas kernels, return_rows(): pl.pallas_call(kernel, out_shape=jax.ShapeDtypeStruct((tok, D), jnp.bfloa...  43 us
    pallas_call x1, Pallas kernels, send_rows(): pl.pallas_call(kernel, out_shape=jax.ShapeDtypeStruct((2, n_sp, rows, D),...  40.2 us
    pallas_call x1, Pallas kernels, first_exchange(): pl.pallas_call(kernel, out_shape=(jax.ShapeDtypeStruct((n_sp,) + bundle.s...  32.2 us
    pallas_call x1, Pallas kernels, group_move(): pl.pallas_call(kernel, out_shape=jax.ShapeDtypeStruct((2, count) + block,...  19.8 us
    unnamed x28, local copies, waits for them, and re-layouts  5.64 us
    dot_general x1, matrix products, shards(): jnp.dot(row_block, expert_gate[0], preferred_element_type=jnp.float32)  3.89 us
    reduce_sum x4, other arithmetic, rms_scale(): jnp.mean(values * values, axis=-1, keepdims=True) + epsilon  3.82 us

profile of v2, /device:TPU:0, one launch (start us, length us, event | category | flops | bytes accessed | tf_op | source)
XLA Modules:
  0.0 176.7 jit_solution(13476527789975152138)
XLA Ops:
  0.1 0.8 convert_element_type.100
  1.1 1.2 fusion.21
  2.3 1.0 fusion.28
  3.5 0.8 copy.45
  4.3 0.7 maximum_maximum_fusion.meta_ref
  5.2 0.8 broadcast_in_dim.42
  5.9 1.5 convolution_convert_fusion.1
  8.3 0.8 pad_maximum_fusion.1.kv_ref
  9.1 32.2 %first_exchange.1 = (bf16[4,2,160,512]{3,2,1,0:T(8,128)(2,1)S(1)}, bf16[2,4,64,2048]{3,2,1,0:T(8,128)(2,1)}, f32[2,4,64,128]{3,2,1,0:T(8,128)}) custom-call(bf16[2,160,512]{2,1,0:T(8,128)(2,1)} %pad_maximum_fusion.1.kv_ref, bf16[64,2048]{1,0:T(8,128)(2,1)} %res_ref.1, f32[64,128]{1,0:T(8,128)} %maximum_maximum_fusion.meta_ref), custom_call_target="tpu_custom_call" | custom-call | tf_op jit(solution)/shard_map/first_exchange/pallas_call | solution.py:189
  41.3 0.9 dynamic-slice_bitcast_fusion.1
  42.3 2.6 %while.18 = (s32[]{:T(128)}, f32[2,512]{1,0:T(2,128)S(1)}, f32[2,512]{1,0:T(2,128)S(1)}, f32[2,512,64]{1,2,0:T(8,128)S(1)}, s32[]{:T(128)}, /*index=5*/bf16[4,2,...) while((s32[]{:T(128)}, f32[2,512]{1,0:T(2,128)S(1)}, ...), condition=%wide.region_11.12_spmd.clone, body=%wide.region_6.11_spmd.clone.sunk | while | flops 174984192 | bytes 9122101 | solution.py:515
  42.3 2.3 %conditional.3 = ((f32[2,512]{1,0:T(2,128)S(1)}, f32[2,512]{1,0:T(2,128)S(1)}, f32[2,512,64]{1,2,0:T(8,128)S(1)})) conditional(s32[]{:T(128)} %convert_element_type.165, (f32[2,512]{1,0:T(2,128)S(1)}, f32[2,512]{1,0:T(2,128)S(1)}, f32[2,512,64]{1,2,0:T(8,128)S(1)}) %tuple.53, (s32[]{:T(128)}, s32[]{:T(128)}, s32[]{:T(128)}, ...), branch_computations={%region_7.7_spmd, %region_8.10_spmd} | conditional | flops 174984192 | bytes 9119822 | solution.py:513
  42.6 0.6 fusion.2
  43.3 0.6 fusion.4
  43.9 0.8 convolution_add_fusion
  44.9 0.8 copy.50.x_ref
  47.7 1.0 copy.53
  48.9 19.8 %gather_heads.1 = bf16[2,4,512,128]{3,2,1,0:T(8,128)(2,1)} custom-call(bf16[512,128]{1,0:T(8,128)(2,1)} %copy.50.x_ref), custom_call_target="tpu_custom_call" | custom-call | tf_op jit(solution)/shard_map/gather_heads/pallas_call | solution.py:147
  68.7 1.5 fusion.17
  70.2 2.7 %convert_bitcast_fusion.1 = f32[512,4,2,128]{3,0,1,2:T(8,128)} fusion(bf16[2,4,512,128]{3,2,1,0:T(8,128)(2,1)} %gather_heads.1), kind=kLoop, calls=%fused_computation.30 | loop fusion | flops 524288 | bytes 3145728 | tf_op jit(solution)/shard_map/convert_element_type | solution.py:520
  72.9 1.9 %copy.51 = f32[512,4,2,128]{0,3,2,1:T(8,128)S(1)} copy(f32[512,4,2,128]{3,0,1,2:T(8,128)} %convert_bitcast_fusion.1) | data formatting | bytes 4194304 | tf_op jit(solution)/shard_map/convert_element_type | solution.py:520
  75.1 1.3 copy-done.2
  76.4 0.5 convert_bitcast_fusion
  77.5 1.7 copy-done.9
  79.1 2.6 %multiply_reduce_fusion = (f32[512]{0:T(512)S(1)}, f32[512,2048]{1,0:T(8,128)S(1)}) fusion(bf16[512,1024]{0,1:T(8,128)(2,1)S(1)} %fusion.19, bf16[1024,2048]{1,0:T(8,128)(2,1)S(1)} %copy-done.9, f32[4,2,64,2048]{3,2,1,0:T(8,128)S(1)} %copy.49), kind=kOutput, calls=%fused_computation.26 | convolution fusion | flops 2150628864 | bytes 13633536 | tf_op jit(solution)/shard_map/dot_general | solution.py:523
  81.8 0.8 constant_dynamic-slice_fusion.1.mid_ref
  83.2 2.2 %convolution_convert_fusion = bf16[576,2048]{1,0:T(8,128)(2,1)} fusion(bf16[256,576]{0,1:T(8,128)(2,1)S(1)} %fusion.27, bf16[256,2048]{1,0:T(8,128)(2,1)S(1)} %bitcast.73), kind=kOutput, calls=%fused_computation.27 | convolution fusion | flops 605159424 | bytes 3702784 | tf_op jit(solution)/shard_map/ts,td->sd/dot_general | solution.py:549
  85.4 40.2 %send_rows.1 = bf16[2,4,144,2048]{3,2,1,0:T(8,128)(2,1)} custom-call(bf16[4,144,2048]{2,1,0:T(8,128)(2,1)} %bitcast.69), custom_call_target="tpu_custom_call" | custom-call | tf_op jit(solution)/shard_map/send_rows/pallas_call | solution.py:268
  125.6 3.9 %fusion.25 = f32[1152,256]{1,0:T(8,128)S(1)} fusion(bf16[1152,2048]{1,0:T(8,128)(2,1)} %bitcast.71, bf16[1,2048,256]{2,1,0:T(8,128)(2,1)S(1)} %copy-done), kind=kOutput, calls=%fused_computation.47 | convolution fusion | flops 1207959552 | bytes 6946816 | tf_op jit(solution)/shard_map/dot_general | solution.py:555
  129.7 2.3 %fusion.16 = bf16[1152,256]{1,0:T(8,128)(2,1)} fusion(bf16[1152,2048]{1,0:T(8,128)(2,1)S(1)} %bitcast.72, f32[1152,256]{1,0:T(8,128)S(1)} %fusion.25, bf16[1,2048,256]{2,1,0:T(8,128)(2,1)S(1)} %copy-done.10), kind=kOutput, calls=%fused_computation.31 | convolution fusion | flops 1209729024 | bytes 7536640 | tf_op jit(solution)/shard_map/dot_general | solution.py:556
  132.0 43.0 %return_rows.1 = bf16[64,2048]{1,0:T(8,128)(2,1)} custom-call(bf16[2,4,144,256]{3,2,1,0:T(8,128)(2,1)} %bitcast.79, bf16[256,2048]{1,0:T(8,128)(2,1)} %bitcast.76, bf16[4,256,144]{2,1,0:T(8,128)(2,1)} %bitcast.74, f32[64,2048]{1,0:T(8,128)} %constant_dynamic-slice_fusion.1.mid_ref), custom_call_target="tpu_custom_call" | custom-call | tf_op jit(solution)/shard_map/return_rows/pallas_call | solution.py:370
  175.0 1.7 copy.75
  (80 shorter events, 5.4 us)
Async XLA Ops:
  0.0 125.6 %copy-start = (bf16[1,2048,256]{2,1,0:T(8,128)(2,1)S(1)}, bf16[1,2048,256]{2,1,0:T(8,128)(2,1)}, u32[]{:S(2)}) copy-start(bf16[1,2048,256]{2,1,0:T(8,128)(2,1)} %param.35) | copy-start | bytes 3145732
  0.0 7.4 %copy-start.4 = (bf16[512,512]{1,0:T(8,128)(2,1)S(1)}, bf16[512,512]{1,0:T(8,128)(2,1)}, u32[]{:S(2)}) copy-start(bf16[512,512]{1,0:T(8,128)(2,1)} %param.22) | copy-start | bytes 1572868
  0.0 7.5 %copy-start.12 = (f32[512]{0:T(512)S(1)}, f32[512]{0:T(512)}, u32[]{:S(2)}) copy-start(f32[512]{0:T(512)} %param.24) | copy-start | bytes 6148
  0.0 8.0 %copy-start.7 = (f32[96]{0:T(128)S(1)}, f32[96]{0:T(128)}, u32[]{:S(2)}) copy-start(f32[96]{0:T(128)} %param.28) | copy-start | bytes 1156
  0.0 7.5 %copy-start.11 = (bf16[512,128]{1,0:T(8,128)(2,1)S(1)}, bf16[512,128]{1,0:T(8,128)(2,1)}, u32[]{:S(2)}) copy-start(bf16[512,128]{1,0:T(8,128)(2,1)} %param.25) | copy-start | bytes 393220
  2.3 5.8 %copy-start.3 = (bf16[512,192]{0,1:T(8,128)(2,1)S(1)}, bf16[512,192]{0,1:T(8,128)(2,1)}, u32[]{:S(2)}) copy-start(bf16[512,192]{0,1:T(8,128)(2,1)} %param.21) | copy-start | bytes 589828
  2.3 5.8 %copy-start.8 = (f32[96]{0:T(128)S(1)}, f32[96]{0:T(128)}, u32[]{:S(2)}) copy-start(f32[96]{0:T(128)} %param.27) | copy-start | bytes 1156
  72.9 2.0 %copy-start.6 = (f32[1024]{0:T(1024)S(1)}, f32[1024]{0:T(1024)}, u32[]{:S(2)}) copy-start(f32[1024]{0:T(1024)} %param.29) | copy-start | bytes 12292
  74.8 1.6 copy-start.2
  77.0 2.2 %copy-start.9 = (bf16[1024,2048]{1,0:T(8,128)(2,1)S(1)}, bf16[1024,2048]{1,0:T(8,128)(2,1)}, u32[]{:S(2)}) copy-start(bf16[1024,2048]{1,0:T(8,128)(2,1)} %param.30) | copy-start | bytes 12582916
  79.1 3.5 %copy-start.5 = (f32[2048]{0:T(1024)S(1)}, f32[2048]{0:T(1024)}, u32[]{:S(2)}) copy-start(f32[2048]{0:T(1024)} %param.32) | copy-start | bytes 24580
  125.6 3.9 %copy-start.1 = (bf16[2,4,144,2048]{3,2,1,0:T(8,128)(2,1)S(1)}, bf16[2,4,144,2048]{3,2,1,0:T(8,128)(2,1)}, u32[]{:S(2)}) copy-start(bf16[2,4,144,2048]{3,2,1,0:T(8,128)(2,1)} %send_rows.1) | copy-start | bytes 14155780
  125.6 4.1 %copy-start.10 = (bf16[1,2048,256]{2,1,0:T(8,128)(2,1)S(1)}, bf16[1,2048,256]{2,1,0:T(8,128)(2,1)}, u32[]{:S(2)}) copy-start(bf16[1,2048,256]{2,1,0:T(8,128)(2,1)} %param.36) | copy-start | bytes 3145732

commit v3 on v2

--- a/solution.py
+++ b/solution.py
@@ -72,135 +72,97 @@
     )
 
 
-class GroupMove:
-    def __init__(self, place, axis, scatter, x_ref, o_ref, sems):
-        self.place, self.axis, self.scatter = place, axis, scatter
-        self.x_ref, self.o_ref = x_ref, o_ref
-        self.local_sem, self.ss, self.rs, self.ps, self.pr = sems
-        self.count = place.n_sp if axis == "sp" else place.n_z
-        self.me = place.sp if axis == "sp" else place.z
-
-    def start(self):
-        p, core = self.place, self.place.core
-        peer, to_id = (p.sp_peer, p.sp_id) if self.axis == "sp" else (p.z_peer, p.z_id)
-        own = self.x_ref.at[self.me] if self.scatter else self.x_ref
-        self.copies = []
-        for step in range(1, self.count):
-            dst = peer(step)
-            src = self.x_ref.at[dst] if self.scatter else self.x_ref
-            copy = remote(
-                src,
-                self.o_ref.at[core, self.me],
-                self.ss.at[step],
-                self.rs.at[step],
-                to_id(dst),
-            )
-            copy.start()
-            self.copies.append(copy)
-        self.local = pltpu.make_async_copy(own, self.o_ref.at[core, self.me], self.local_sem.at[0])
-        self.local.start()
-        self.relays = [
-            remote(
-                own, self.o_ref.at[core, self.me], self.ps.at[0], self.pr.at[0], p.partner()
-            )
-        ]
-        self.relays[0].start()
-
-    def relay(self):
-        core = self.place.core
-        for step in range(1, self.count):
-            src = lax.rem(self.me - step + self.count, self.count)
-            self.copies[step - 1].wait_recv()
-            block = self.o_ref.at[core, src]
-            copy = remote(block, block, self.ps.at[step], self.pr.at[step], self.place.partner())
-            copy.start()
-            self.relays.append(copy)
-
-    def finish(self):
-        for copy in self.copies:
-            copy.wait_send()
-        for copy in self.relays:
-            copy.wait()
-        self.local.wait()
-
-
-def move_sems(count):
-    return [pltpu.SemaphoreType.DMA((1,))] + [pltpu.SemaphoreType.DMA((count,))] * 4
-
-
 def vmem():
     return pl.BlockSpec(memory_space=pltpu.VMEM)
 
 
-def group_move(x, axis, scatter, n_sp, n_z, collective_id, name):
-    count = n_sp if axis == "sp" else n_z
-    block = x.shape[1:] if scatter else x.shape
-
-    def kernel(x_ref, o_ref, *sems):
+def gather_heads(x, n_sp, n_z):
+    n_tp = 2 * n_z
+
+    def kernel(x_ref, o_ref, local_sem, send_sem, recv_sem):
         place = Place(n_sp, n_z)
-        place.barrier(axis == "sp", axis == "z")
-        move = GroupMove(place, axis, scatter, x_ref, o_ref, sems)
-        move.start()
-        move.relay()
-        move.finish()
-
-    return pl.pallas_call(
-        kernel,
-        out_shape=jax.ShapeDtypeStruct((2, count) + block, x.dtype),
-        in_specs=[vmem()],
-        out_specs=vmem(),
-        scratch_shapes=move_sems(count),
-        compiler_params=pltpu.CompilerParams(
-            collective_id=collective_id, has_side_effects=True, vmem_limit_bytes=60 << 20
-        ),
-        name=name,
-    )(x)
-
-
-def first_exchange(bundle, residual, meta, n_sp, n_z):
-    def kernel(kv_ref, res_ref, meta_ref, kv_out, res_out, meta_out, kv_local, kv_s, kv_r, *sems):
-        place = Place(n_sp, n_z)
-        place.barrier(True, True)
+        sem = pltpu.get_barrier_semaphore()
+        for step in range(1, n_tp):
+            pl.semaphore_signal(
+                sem,
+                inc=1,
+                device_id=(place.sp, lax.rem(place.tp + step, n_tp)),
+                device_id_type=MESH_ID,
+            )
+        pl.semaphore_wait(sem, n_tp - 1)
         copies = []
-        for step in range(1, n_sp):
+        for step in range(1, n_tp):
+            dst = lax.rem(place.tp + step, n_tp)
             copy = remote(
-                kv_ref,
-                kv_out.at[place.sp],
-                kv_s.at[step],
-                kv_r.at[step],
-                place.sp_id(place.sp_peer(step)),
+                x_ref.at[lax.rem(dst, 2)],
+                o_ref.at[place.tp],
+                send_sem.at[step],
+                recv_sem.at[step],
+                (place.sp, dst),
             )
             copy.start()
             copies.append(copy)
-        local = pltpu.make_async_copy(kv_ref, kv_out.at[place.sp], kv_local.at[0])
+        local = pltpu.make_async_copy(x_ref.at[place.core], o_ref.at[place.tp], local_sem.at[0])
         local.start()
-        meta_move = GroupMove(place, "z", False, meta_ref, meta_out, sems[:5])
-        res_move = GroupMove(place, "z", False, res_ref, res_out, sems[5:])
-        meta_move.start()
-        res_move.start()
-        meta_move.relay()
-        res_move.relay()
         for copy in copies:
             copy.wait()
         local.wait()
-        meta_move.finish()
-        res_move.finish()
-
+
+    return pl.pallas_call(
+        kernel,
+        out_shape=jax.ShapeDtypeStruct((n_tp,) + x.shape[1:], x.dtype),
+        in_specs=[vmem()],
+        out_specs=vmem(),
+        scratch_shapes=[
+            pltpu.SemaphoreType.DMA((1,)),
+            pltpu.SemaphoreType.DMA((n_tp,)),
+            pltpu.SemaphoreType.DMA((n_tp,)),
+        ],
+        compiler_params=pltpu.CompilerParams(
+            collective_id=1, has_side_effects=True, vmem_limit_bytes=60 << 20
+        ),
+        name="gather_heads",
+    )(x)
+
+
+def first_exchange(bundle, residual, meta, n_sp, n_z):
+    def kernel(kv_ref, res_ref, meta_ref, kv_out, res_out, meta_out, local_sem, *sems):
+        place = Place(n_sp, n_z)
+        place.barrier(True, True)
+        moves = (
+            (meta_ref, meta_out, n_z, place.z, place.z_peer, place.z_id),
+            (res_ref, res_out, n_z, place.z, place.z_peer, place.z_id),
+            (kv_ref, kv_out, n_sp, place.sp, place.sp_peer, place.sp_id),
+        )
+        copies = []
+        for number, (src, out, count, me, peer, to_id) in enumerate(moves):
+            for step in range(1, count):
+                copy = remote(
+                    src,
+                    out.at[me],
+                    sems[2 * number].at[step],
+                    sems[2 * number + 1].at[step],
+                    to_id(peer(step)),
+                )
+                copy.start()
+                copies.append(copy)
+            local = pltpu.make_async_copy(src, out.at[me], local_sem.at[number])
+            local.start()
+            copies.append(local)
+        for copy in copies:
+            copy.wait()
+
+    dma = pltpu.SemaphoreType.DMA
     return pl.pallas_call(
         kernel,
         out_shape=(
             jax.ShapeDtypeStruct((n_sp,) + bundle.shape, bundle.dtype),
-            jax.ShapeDtypeStruct((2, n_z) + residual.shape, residual.dtype),
-            jax.ShapeDtypeStruct((2, n_z) + meta.shape, meta.dtype),
+            jax.ShapeDtypeStruct((n_z,) + residual.shape, residual.dtype),
+            jax.ShapeDtypeStruct((n_z,) + meta.shape, meta.dtype),
         ),
         in_specs=[vmem()] * 3,
         out_specs=(vmem(),) * 3,
-        scratch_shapes=[
-            pltpu.SemaphoreType.DMA((1,)),
-            pltpu.SemaphoreType.DMA((n_sp,)),
-            pltpu.SemaphoreType.DMA((n_sp,)),
-        ]
-        + move_sems(n_z) * 2,
+        scratch_shapes=[dma((3,))] + [dma((n_z,))] * 4 + [dma((n_sp,))] * 2,
         compiler_params=pltpu.CompilerParams(
             collective_id=0, has_side_effects=True, vmem_limit_bytes=60 << 20
         ),
@@ -514,25 +476,25 @@
 
     row_peak, row_total, weighted = lax.fori_loop(0, block_count, one_block, init_state)
     attended = (weighted / row_total[..., None]).astype(jnp.bfloat16)
-    head_major = jnp.transpose(attended, (1, 0, 2)).reshape(shard_len, local_heads * VH)
-    gathered = group_move(head_major, "z", False, sp_count, z_count, 1, "gather_heads")
-    att_rows = (
-        jnp.transpose(gathered, (2, 1, 0, 3)).reshape(shard_len, -1).astype(jnp.float32)
-    )
+    part_len = z_count * tok_count
+    by_core = (
+        attended.reshape(local_heads, z_count, 2, tok_count, VH)
+        .transpose(2, 1, 3, 0, 4)
+        .reshape(2, part_len, local_heads * VH)
+    )
+    gathered = gather_heads(by_core, sp_count, z_count)
+    att_rows = jnp.transpose(gathered, (1, 0, 2)).reshape(part_len, -1).astype(jnp.float32)
     normed_rows = (att_rows * rms_scale(att_rows) * out_gain).astype(jnp.bfloat16)
     mixed = jnp.dot(normed_rows, out_weight, preferred_element_type=jnp.float32)
-    residual_rows = jnp.transpose(residual_all, (1, 0, 2, 3)).reshape(shard_len, D)
-    middle = residual_rows.astype(jnp.float32) + mixed
-    ffn_input = (middle * rms_scale(middle) * ffn_gain).astype(jnp.bfloat16)
+    middle = residual_all.reshape(part_len, D).astype(jnp.float32) + mixed
+    part_input = (middle * rms_scale(middle) * ffn_gain).astype(jnp.bfloat16)
     own_middle = lax.dynamic_slice_in_dim(
-        middle, lax.axis_index("tp") * tok_count, tok_count, 0
+        middle, lax.axis_index("tp") // 2 * tok_count, tok_count, 0
     )
     slot_cap = max(2, 9 * tok_count * TOPK // (8 * sp_count))
     rows = z_count * slot_cap
-    core = lax.axis_index("tp") % 2
-    part_meta = lax.dynamic_index_in_dim(meta_all, core, 0, keepdims=False)
-    part_routes = part_meta[:, :, :TOPK].astype(jnp.int32).reshape(z_count, tok_count * TOPK)
-    part_weights = part_meta[:, :, TOPK : 2 * TOPK].reshape(z_count * tok_count, TOPK)
+    part_routes = meta_all[:, :, :TOPK].astype(jnp.int32).reshape(z_count, tok_count * TOPK)
+    part_weights = meta_all[:, :, TOPK : 2 * TOPK].reshape(z_count * tok_count, TOPK)
     one_hot = (part_routes[:, :, None] == jnp.arange(sp_count, dtype=jnp.int32)).astype(jnp.int32)
     earlier = jnp.cumsum(one_hot, axis=1) - one_hot
     rank_in = jnp.sum(earlier * one_hot, axis=2)
@@ -542,9 +504,6 @@
     chooser = jnp.sum(hits.astype(jnp.bfloat16), axis=1)
     mixer = jnp.sum(jnp.where(hits, part_weights[:, :, None], 0.0), axis=1).astype(jnp.bfloat16)
     mixer = jnp.transpose(mixer.reshape(z_count * tok_count, sp_count, rows), (1, 0, 2))
-    part_input = lax.dynamic_index_in_dim(
-        ffn_input.reshape(z_count, 2, tok_count, D), core, 1, keepdims=False
-    ).reshape(z_count * tok_count, D)
     outbound = (
         jnp.einsum("ts,td->sd", chooser, part_input, preferred_element_type=jnp.float32)
         .astype(jnp.bfloat16)

time: 177 us -> 167 us (0.944)
  local copies, waits for them, and re-layouts: 13.8 us -> 9.3 us
  Pallas kernels: 135 us -> 131 us
  other arithmetic: 12.6 us -> 9.79 us
    pallas_call x1, Pallas kernels: 19.8 us -> 17.1 us  [gather_heads(): pl.pallas_call(kernel, out_shape=jax.ShapeDtypeStruct((n_tp,) + x.shape[1...]
    convert_element_type x3 -> x1, other arithmetic: 3.58 us -> 1.12 us  [shards(): jnp.transpose(gathered, (1, 0, 2)).reshape(part_len, -1).astype(jnp.float32)]
    pallas_call x1, Pallas kernels: 32.2 us -> 30.1 us  [first_exchange(): pl.pallas_call(kernel, out_shape=(jax.ShapeDtypeStruct((n_sp,) + bundle.s...]
    convert_element_type x3 -> x2, local copies, waits for them, and re-layouts: 2.94 us -> 0.84 us  [the longest x1 0.51 us: shards(): meta_all[:, :, :TOPK].astype(jnp.int32).reshape(z_count, tok_count * TOPK)]
    unnamed x28, local copies, waits for them, and re-layouts: 5.64 us -> 3.64 us
where the time goes in v3:
time: 167 us; the launch traced here: 166 us
  Pallas kernels  131 us (78%)
  matrix products  15.5 us (9%)
  other arithmetic  9.79 us (6%)
  local copies, waits for them, and re-layouts  9.3 us (6%)
    pallas_call x1, Pallas kernels, return_rows(): pl.pallas_call(kernel, out_shape=jax.ShapeDtypeStruct((tok, D), jnp.bfloa...  42.7 us
    pallas_call x1, Pallas kernels, send_rows(): pl.pallas_call(kernel, out_shape=jax.ShapeDtypeStruct((2, n_sp, rows, D),...  41.3 us
    pallas_call x1, Pallas kernels, first_exchange(): pl.pallas_call(kernel, out_shape=(jax.ShapeDtypeStruct((n_sp,) + bundle.s...  30.1 us
    pallas_call x1, Pallas kernels, gather_heads(): pl.pallas_call(kernel, out_shape=jax.ShapeDtypeStruct((n_tp,) + x.shape[1...  17.1 us
    dot_general x1, matrix products, shards(): jnp.dot(row_block, expert_gate[0], preferred_element_type=jnp.float32)  3.89 us
    unnamed x28, local copies, waits for them, and re-layouts  3.64 us
    dot_general x1, matrix products, shards(): mixed = jnp.dot(normed_rows, out_weight, preferred_element_type=jnp.float32)  3.58 us
    reduce_sum x4, other arithmetic, rms_scale(): jnp.mean(values * values, axis=-1, keepdims=True) + epsilon  3.54 us

profile of v3, /device:TPU:0, one launch (start us, length us, event | category | flops | bytes accessed | tf_op | source)
XLA Modules:
  0.0 166.4 jit_solution(6021606868210834373)
XLA Ops:
  0.1 0.8 convert_element_type.97
  1.1 1.2 fusion.18
  2.3 1.0 fusion.30
  3.5 0.8 copy.32
  4.3 0.7 maximum_maximum_fusion.meta_ref
  5.2 0.8 broadcast_in_dim.42
  5.9 1.5 convolution_convert_fusion.1
  7.5 0.4 bitcast_convert_fusion
  8.3 0.8 pad_maximum_fusion.1.kv_ref
  9.1 30.1 %first_exchange.1 = (bf16[4,2,160,512]{3,2,1,0:T(8,128)(2,1)S(1)}, bf16[4,64,2048]{2,1,0:T(8,128)(2,1)}, f32[4,64,128]{2,1,0:T(8,128)}) custom-call(bf16[2,160,512]{2,1,0:T(8,128)(2,1)} %pad_maximum_fusion.1.kv_ref, bf16[64,2048]{1,0:T(8,128)(2,1)} %res_ref.1, f32[64,128]{1,0:T(8,128)} %maximum_maximum_fusion.meta_ref), custom_call_target="tpu_custom_call" | custom-call | tf_op jit(solution)/shard_map/first_exchange/pallas_call | solution.py:156
  39.2 2.6 %while.18 = (s32[]{:T(128)}, f32[2,512]{1,0:T(2,128)S(1)}, f32[2,512]{1,0:T(2,128)S(1)}, f32[2,512,64]{1,2,0:T(8,128)S(1)}, s32[]{:T(128)}, /*index=5*/bf16[4,2,...) while((s32[]{:T(128)}, f32[2,512]{1,0:T(2,128)S(1)}, ...), condition=%wide.region_11.12_spmd.clone, body=%wide.region_6.11_spmd.clone.sunk | while | flops 174984192 | bytes 9122101 | solution.py:477
  39.3 2.3 %conditional.3 = ((f32[2,512]{1,0:T(2,128)S(1)}, f32[2,512]{1,0:T(2,128)S(1)}, f32[2,512,64]{1,2,0:T(8,128)S(1)})) conditional(s32[]{:T(128)} %convert_element_type.160, (f32[2,512]{1,0:T(2,128)S(1)}, f32[2,512]{1,0:T(2,128)S(1)}, f32[2,512,64]{1,2,0:T(8,128)S(1)}) %tuple.53, (s32[]{:T(128)}, s32[]{:T(128)}, s32[]{:T(128)}, ...), branch_computations={%region_7.7_spmd, %region_8.10_spmd} | conditional | flops 174984192 | bytes 9119822 | solution.py:475
  39.6 0.6 fusion.2
  40.2 0.6 fusion.4
  40.8 0.8 convolution_add_fusion
  42.0 0.4 copy.36
  42.4 0.8 reshape.223.x_ref
  43.4 0.5 copy.33
  45.3 1.0 copy.39
  46.5 17.1 %gather_heads.1 = bf16[8,256,128]{2,1,0:T(8,128)(2,1)} custom-call(bf16[2,256,128]{2,1,0:T(8,128)(2,1)} %reshape.223.x_ref), custom_call_target="tpu_custom_call" | custom-call | tf_op jit(solution)/shard_map/gather_heads/pallas_call | solution.py:111
  63.6 1.2 fusion.21
  64.8 1.1 convert_bitcast_fusion
  65.9 0.3 copy.37
  66.5 1.0 copy-done.3
  67.5 3.6 %multiply_reduce_fusion = (f32[256]{0:T(256)S(1)}, f32[256,2048]{1,0:T(8,128)S(1)}) fusion(bf16[256,1024]{0,1:T(8,128)(2,1)S(1)} %fusion.26, bf16[1024,2048]{1,0:T(8,128)(2,1)} %param.30, bf16[256,2048]{1,0:T(8,128)(2,1)S(1)} %bitcast.68), kind=kOutput, calls=%fused_computation.28 | convolution fusion | flops 1075838720 | bytes 7865344 | tf_op jit(solution)/shard_map/dot_general | solution.py:488
  71.1 0.8 constant_dynamic-slice_fusion.mid_ref
  72.0 2.4 %convolution_convert_fusion = bf16[576,2048]{1,0:T(8,128)(2,1)} fusion(bf16[256,576]{0,1:T(8,128)(2,1)S(1)} %fusion.29, f32[256,2048]{1,0:T(8,128)S(1)} %get-tuple-element.250, f32[2048]{0:T(1024)S(1)} %copy-done.6, f32[256]{0:T(256)S(1)} %add_rsqrt_fusion.3), kind=kOutput, calls=%fused_computation.23 | convolution fusion | flops 606732288 | bytes 4760576 | tf_op jit(solution)/shard_map/ts,td->sd/dot_general | solution.py:508
  74.3 41.3 %send_rows.1 = bf16[2,4,144,2048]{3,2,1,0:T(8,128)(2,1)} custom-call(bf16[4,144,2048]{2,1,0:T(8,128)(2,1)} %bitcast.62), custom_call_target="tpu_custom_call" | custom-call | tf_op jit(solution)/shard_map/send_rows/pallas_call | solution.py:230
  115.7 3.9 %fusion.23 = f32[1152,256]{1,0:T(8,128)S(1)} fusion(bf16[1152,2048]{1,0:T(8,128)(2,1)} %bitcast.63, bf16[1,2048,256]{2,1,0:T(8,128)(2,1)S(1)} %copy-done), kind=kOutput, calls=%fused_computation.43 | convolution fusion | flops 1207959552 | bytes 6946816 | tf_op jit(solution)/shard_map/dot_general | solution.py:514
  119.8 2.3 %fusion.16 = bf16[1152,256]{1,0:T(8,128)(2,1)} fusion(bf16[1152,2048]{1,0:T(8,128)(2,1)S(1)} %bitcast.64, f32[1152,256]{1,0:T(8,128)S(1)} %fusion.23, bf16[1,2048,256]{2,1,0:T(8,128)(2,1)S(1)} %copy-done.10), kind=kOutput, calls=%fused_computation.26 | convolution fusion | flops 1209729024 | bytes 7536640 | tf_op jit(solution)/shard_map/dot_general | solution.py:515
  122.1 42.7 %return_rows.1 = bf16[64,2048]{1,0:T(8,128)(2,1)} custom-call(bf16[2,4,144,256]{3,2,1,0:T(8,128)(2,1)} %bitcast.72, bf16[256,2048]{1,0:T(8,128)(2,1)} %bitcast.67, bf16[4,256,144]{2,1,0:T(8,128)(2,1)} %bitcast.65, f32[64,2048]{1,0:T(8,128)} %constant_dynamic-slice_fusion.mid_ref), custom_call_target="tpu_custom_call" | custom-call | tf_op jit(solution)/shard_map/return_rows/pallas_call | solution.py:332
  164.8 1.7 %copy.60 = bf16[64,2048]{1,0:T(8,128)(2,1)} copy(bf16[64,2048]{1,0:T(8,128)(2,1)} %return_rows.1) | data formatting | bytes 524288
  (77 shorter events, 3.6 us)
Async XLA Ops:
  0.0 115.7 %copy-start = (bf16[1,2048,256]{2,1,0:T(8,128)(2,1)S(1)}, bf16[1,2048,256]{2,1,0:T(8,128)(2,1)}, u32[]{:S(2)}) copy-start(bf16[1,2048,256]{2,1,0:T(8,128)(2,1)} %param.35) | copy-start | bytes 3145732
  0.0 7.5 %copy-start.5 = (bf16[512,512]{1,0:T(8,128)(2,1)S(1)}, bf16[512,512]{1,0:T(8,128)(2,1)}, u32[]{:S(2)}) copy-start(bf16[512,512]{1,0:T(8,128)(2,1)} %param.22) | copy-start | bytes 1572868
  0.0 7.5 %copy-start.12 = (f32[512]{0:T(512)S(1)}, f32[512]{0:T(512)}, u32[]{:S(2)}) copy-start(f32[512]{0:T(512)} %param.24) | copy-start | bytes 6148
  0.0 8.0 %copy-start.8 = (f32[96]{0:T(128)S(1)}, f32[96]{0:T(128)}, u32[]{:S(2)}) copy-start(f32[96]{0:T(128)} %param.28) | copy-start | bytes 1156
  0.0 7.5 %copy-start.11 = (bf16[512,128]{1,0:T(8,128)(2,1)S(1)}, bf16[512,128]{1,0:T(8,128)(2,1)}, u32[]{:S(2)}) copy-start(bf16[512,128]{1,0:T(8,128)(2,1)} %param.25) | copy-start | bytes 393220
  2.3 5.8 %copy-start.4 = (bf16[512,192]{0,1:T(8,128)(2,1)S(1)}, bf16[512,192]{0,1:T(8,128)(2,1)}, u32[]{:S(2)}) copy-start(bf16[512,192]{0,1:T(8,128)(2,1)} %param.21) | copy-start | bytes 589828
  2.3 5.8 %copy-start.9 = (f32[96]{0:T(128)S(1)}, f32[96]{0:T(128)}, u32[]{:S(2)}) copy-start(f32[96]{0:T(128)} %param.27) | copy-start | bytes 1156
  39.2 4.0 %copy-start.2 = (f32[4,64,128]{2,1,0:T(8,128)S(1)}, f32[4,64,128]{2,1,0:T(8,128)}, u32[]{:S(2)}) copy-start(f32[4,64,128]{2,1,0:T(8,128)} %get-tuple-element.187) | copy-start | bytes 393220
  63.6 2.7 %copy-start.7 = (f32[1024]{0:T(1024)S(1)}, f32[1024]{0:T(1024)}, u32[]{:S(2)}) copy-start(f32[1024]{0:T(1024)} %param.29) | copy-start | bytes 12292
  66.3 1.2 copy-start.3
  67.5 4.4 %copy-start.6 = (f32[2048]{0:T(1024)S(1)}, f32[2048]{0:T(1024)}, u32[]{:S(2)}) copy-start(f32[2048]{0:T(1024)} %param.32) | copy-start | bytes 24580
  115.7 3.9 %copy-start.1 = (bf16[2,4,144,2048]{3,2,1,0:T(8,128)(2,1)S(1)}, bf16[2,4,144,2048]{3,2,1,0:T(8,128)(2,1)}, u32[]{:S(2)}) copy-start(bf16[2,4,144,2048]{3,2,1,0:T(8,128)(2,1)} %send_rows.1) | copy-start | bytes 14155780
  115.7 4.1 %copy-start.10 = (bf16[1,2048,256]{2,1,0:T(8,128)(2,1)S(1)}, bf16[1,2048,256]{2,1,0:T(8,128)(2,1)}, u32[]{:S(2)}) copy-start(bf16[1,2048,256]{2,1,0:T(8,128)(2,1)} %param.36) | copy-start | bytes 3145732
